TPU v7x, 32 devices: a whole 2x2x4 slice. The times are simulated.
32 devices in a mesh: grp: 2 (over x), ep: 16 (over z, y, core).
Axes of the slice: x: 2, y: 2, z: 4, core: 2. Of those that a mesh axis runs over, the one named last changes fastest.
Arguments:
- hidden: bfloat16 [224, 2048], P(('grp', 'ep')), parts along dimension 0, may hold values from -6 to 6
- state_in: float32 [224, 64, 4096], P(('grp', 'ep')), parts along dimension 0, may hold values from -4 to 4
- conv_state: bfloat16 [224, 3, 4608], P(('grp', 'ep')), parts along dimension 0, may hold values from -6 to 6
- expert_ids: int32 [224, 4], P(('grp', 'ep')), parts along dimension 0, may hold values from 0 to 15, as said below
- group_prob: float32 [224], P(('grp', 'ep')), parts along dimension 0, may hold values from 0.25 to 1
- expert_score: float32 [224, 4], P(('grp', 'ep')), parts along dimension 0, may hold values from 0.05 to 1
- first_gain: bfloat16 [2048], replicated, may hold values from 0.099609375 to 1.8984375
- z_weight: bfloat16 [2048, 4096], P(None, 'ep'), may hold values from -0.125 to 0.125
- x_weight: bfloat16 [2048, 4096], P(None, 'ep'), may hold values from -0.125 to 0.125
- b_weight: bfloat16 [2048, 256], replicated, may hold values from -0.125 to 0.125
- c_weight: bfloat16 [2048, 256], replicated, may hold values from -0.125 to 0.125
- dt_weight: bfloat16 [2048, 64], replicated, may hold values from -0.125 to 0.125
- conv_weight: bfloat16 [4, 4608], replicated, may hold values from -3 to 3
- conv_bias: bfloat16 [4608], replicated, may hold values from -3 to 3
- dt_bias: float32 [64], replicated, may hold values from -4 to 0
- decay_log: float32 [64], replicated, may hold values from 0 to 2
- skip_gain: float32 [64], replicated, may hold values from 0.1 to 1.9
- inner_gain: bfloat16 [4096], replicated, may hold values from 0.099609375 to 1.8984375
- out_weight: bfloat16 [4096, 2048], P(None, 'ep'), may hold values from -0.09375 to 0.09375
- second_gain: bfloat16 [2048], replicated, may hold values from 0.099609375 to 1.8984375
- expert_gate: bfloat16 [16, 2048, 512], P('ep'), may hold values from -0.125 to 0.125
- expert_up: bfloat16 [16, 2048, 512], P('ep'), may hold values from -0.125 to 0.125
- expert_down: bfloat16 [16, 512, 2048], P('ep'), may hold values from -0.25 to 0.25
Outputs:
- layer_out: bfloat16 [224, 2048], P(('grp', 'ep')), parts along dimension 0
- state_out: float32 [224, 64, 4096], P(('grp', 'ep')), parts along dimension 0
- conv_out: bfloat16 [224, 3, 4608], P(('grp', 'ep')), parts along dimension 0
There are 2 independent parts, one for each index of `grp`. A program takes and returns all parts, laid end to end along the dimension named above; an argument that names none is the same for every part. Nothing has to cross between parts.
Inputs may be any that keep to these rules, and one draw needn't show every extreme that they name: `expert_ids`: each row names 4 different experts of one expert group (numbers g * 8 to g * 8 + 7). Among the 7 rows of one device no expert is named more than 3 times, and in every draw one expert is named exactly 3 times by the rows of every device.
All inputs are finite; a program needn't handle non-finite values.
Results may differ from a plain program's by a relative error of at most 0.014.
Values may be sent and summed in bfloat16 or wider, within the bound.
A program may use at most 128 MiB of HBM per device.

v0:
```python
import jax
import jax.numpy as jnp
from jax import lax
from jax.sharding import PartitionSpec as P

HEADS = 64
HEAD_DIM = 64
SSM_GROUPS = 4
STATE = 64
TOP = 4


EPS = 1e-06


def rms_scale(values, gain_vec):
    return (
        values
        * lax.rsqrt(jnp.mean(values * values, axis=-1, keepdims=True) + EPS)
        * gain_vec.astype(jnp.float32)
    )


def state_step(active, dt_raw, state_in, dt_bias, decay_log, skip_gain):
    row_count = active.shape[0]
    inner_width = HEADS * HEAD_DIM
    state_span = SSM_GROUPS * STATE
    per_group = HEADS // SSM_GROUPS
    x_heads = active[:, :inner_width].reshape(row_count, HEADS, HEAD_DIM)
    b_input = active[:, inner_width : inner_width + state_span].reshape(
        row_count, SSM_GROUPS, STATE
    )
    c_input = active[:, inner_width + state_span :].reshape(row_count, SSM_GROUPS, STATE)
    b_heads = jnp.repeat(b_input, per_group, axis=1)
    c_heads = jnp.repeat(c_input, per_group, axis=1)
    step_size = jax.nn.softplus(dt_raw.astype(jnp.float32) + dt_bias[None, :])
    decay_rate = jnp.exp(-step_size * jnp.exp(decay_log)[None, :])
    carried = state_in.reshape(row_count, HEADS, HEAD_DIM, STATE)
    carried = (
        decay_rate[:, :, None, None] * carried
        + (step_size[:, :, None] * x_heads)[:, :, :, None] * b_heads[:, :, None, :]
    )
    readout = jnp.einsum("bhpn,bhn->bhp", carried, c_heads, precision=lax.Precision.HIGHEST)
    readout = readout + skip_gain[None, :, None] * x_heads
    return (
        readout.reshape(row_count, inner_width),
        carried.reshape(row_count, HEADS, HEAD_DIM * STATE),
    )


def body(
    hidden,
    state_in,
    conv_state,
    expert_ids,
    group_prob,
    expert_score,
    first_gain,
    z_weight,
    x_weight,
    b_weight,
    c_weight,
    dt_weight,
    conv_weight,
    conv_bias,
    dt_bias,
    decay_log,
    skip_gain,
    inner_gain,
    out_weight,
    second_gain,
    expert_gate,
    expert_up,
    expert_down,
):
    row_count = hidden.shape[0]
    model_width = hidden.shape[1]
    normed = rms_scale(hidden.astype(jnp.float32), first_gain).astype(jnp.bfloat16)
    row_part = lax.all_gather(normed, "ep", axis=0, tiled=True)
    both_parts = jnp.concatenate(
        [
            jnp.dot(row_part, z_weight, preferred_element_type=jnp.float32),
            jnp.dot(row_part, x_weight, preferred_element_type=jnp.float32),
        ],
        axis=1,
    )
    projected_both = both_parts.astype(jnp.bfloat16)
    col_count = z_weight.shape[1]
    gate_z, x_part = (
        lax.all_to_all(
            projected_both[:, :col_count], "ep", split_axis=0, concat_axis=1, tiled=True
        ),
        lax.all_to_all(
            projected_both[:, col_count:], "ep", split_axis=0, concat_axis=1, tiled=True
        ),
    )
    b_part = jnp.dot(normed, b_weight, preferred_element_type=jnp.float32).astype(jnp.bfloat16)
    c_part = jnp.dot(normed, c_weight, preferred_element_type=jnp.float32).astype(jnp.bfloat16)
    dt_raw = jnp.dot(normed, dt_weight, preferred_element_type=jnp.float32).astype(jnp.bfloat16)
    fresh_input = jnp.concatenate([x_part, b_part, c_part], axis=1)
    window = jnp.concatenate([conv_state, fresh_input[:, None, :]], axis=1)
    summed = jnp.sum(window.astype(jnp.float32) * conv_weight.astype(jnp.float32)[None], axis=1)
    active = jax.nn.silu(summed + conv_bias.astype(jnp.float32)[None, :])
    readout, state_out = state_step(active, dt_raw, state_in, dt_bias, decay_log, skip_gain)
    gated = readout * jax.nn.silu(gate_z.astype(jnp.float32))
    y_mix = rms_scale(gated, inner_gain).astype(jnp.bfloat16)
    slice_out = jnp.dot(
        lax.all_gather(y_mix, "ep", axis=0, tiled=True),
        out_weight,
        preferred_element_type=jnp.float32,
    ).astype(jnp.bfloat16)
    projected = lax.all_to_all(slice_out, "ep", split_axis=0, concat_axis=1, tiled=True)
    projected = lax.optimization_barrier(projected)
    mixed_rows = (hidden.astype(jnp.float32) + projected.astype(jnp.float32)).astype(jnp.bfloat16)
    normed2 = rms_scale(mixed_rows.astype(jnp.float32), second_gain).astype(jnp.bfloat16)
    expert_count = lax.axis_size("ep")
    capacity = max(2, (3 * row_count * TOP + 2 * expert_count - 1) // (2 * expert_count))
    slot_total = expert_count * capacity
    flat_ids = expert_ids.reshape(-1)
    one_hot = (flat_ids[:, None] == jnp.arange(expert_count, dtype=jnp.int32)[None, :]).astype(
        jnp.int32
    )
    earlier = jnp.cumsum(one_hot, axis=0) - one_hot
    slot_rank = jnp.sum(earlier * one_hot, axis=1)
    slot_place = (flat_ids * capacity + slot_rank).reshape(row_count, TOP)
    slot_index = jnp.arange(slot_total, dtype=jnp.int32)
    dispatch = jnp.sum(
        (slot_index[:, None, None] == slot_place[None, :, :]).astype(jnp.int32), axis=2
    )
    outgoing = jnp.dot(dispatch.astype(jnp.bfloat16), normed2, preferred_element_type=jnp.float32)
    outgoing = outgoing.astype(jnp.bfloat16).reshape(expert_count, capacity, model_width)
    arrived = lax.all_to_all(outgoing, "ep", split_axis=0, concat_axis=0, tiled=True)
    sources, slots_here, width = arrived.shape
    flattened = arrived.reshape(sources * slots_here, width)
    gate_part = jnp.dot(flattened, expert_gate[0], preferred_element_type=jnp.float32)
    up_part = jnp.dot(flattened, expert_up[0], preferred_element_type=jnp.float32)
    hidden_act = (jax.nn.silu(gate_part) * up_part).astype(jnp.bfloat16)
    expert_out = jnp.dot(hidden_act, expert_down[0], preferred_element_type=jnp.float32).astype(
        jnp.bfloat16
    )
    returned = lax.all_to_all(
        expert_out.reshape(sources, slots_here, width),
        "ep",
        split_axis=0,
        concat_axis=0,
        tiled=True,
    )
    returned = returned.reshape(slot_total, model_width)
    route_share = group_prob[:, None] * expert_score / jnp.sum(expert_score, axis=1, keepdims=True)
    moe_sum = jnp.zeros((row_count, model_width), jnp.float32)
    for pick in range(TOP):
        select_rows = (slot_place[:, pick][:, None] == slot_index[None, :]).astype(jnp.bfloat16)
        picked = jnp.dot(select_rows, returned, preferred_element_type=jnp.float32)
        moe_sum = moe_sum + route_share[:, pick : pick + 1] * picked
    layer_out = (mixed_rows.astype(jnp.float32) + moe_sum).astype(jnp.bfloat16)
    return (layer_out, state_out, window[:, 1:, :])


def solution(mesh):
    in_specs = (
        P(("grp", "ep"), None),
        P(("grp", "ep"), None, None),
        P(("grp", "ep"), None, None),
        P(("grp", "ep"), None),
        P(("grp", "ep")),
        P(("grp", "ep"), None),
        P(),
        P(None, "ep"),
        P(None, "ep"),
        P(),
        P(),
        P(),
        P(),
        P(),
        P(),
        P(),
        P(),
        P(),
        P(None, "ep"),
        P(),
        P("ep", None, None),
        P("ep", None, None),
        P("ep", None, None),
    )
    out_specs = (P(("grp", "ep"), None), P(("grp", "ep"), None, None), P(("grp", "ep"), None, None))
    return jax.shard_map(body, mesh=mesh, in_specs=in_specs, out_specs=out_specs, check_vma=False)
```

profile of v0, /device:TPU:0, one launch (start us, length us, event | category | flops | bytes accessed | tf_op | source)
XLA Modules:
  0.0 186.1 jit_solution(1612493214570379041)
XLA Ops:
  0.6 0.8 convert_element_type.99
  1.5 0.9 fusion.30
  2.4 0.8 fusion.52
  3.2 24.6 %all-gather = bf16[16,7,2048]{2,1,0:T(8,128)(2,1)S(1)} all-gather(bf16[1,7,2048]{2,1,0:T(8,128)(2,1)S(1)} %fusion.52), channel_id=1, replica_groups=mesh['grp'=2,'ep'=16] {'ep'}, dimensions={0}, use_global_device_ids=true | all-gather | bytes 487424 | tf_op jit(solution)/shard_map/all_gather | solution.py:79
  27.8 0.2 reshape.119
  28.0 1.5 convolution_convert_fusion.3
  29.5 0.7 all_to_all.44
  30.2 3.5 %all-to-all-start = ((bf16[16,7,256]{2,1,0:T(8,128)(2,1)}), bf16[16,7,256]{2,1,0:T(8,128)(2,1)S(1)}, u32[]{:S(2)}, u32[]{:S(2)}) async-start(bf16[16,7,256]{2,1,0:T(8,128)(2,1)} %all_to_all.44), calls=%async_computation | async-start | bytes 131072 | tf_op jit(solution)/shard_map/all_to_all | solution.py:93
  33.7 1.5 convolution_convert_fusion.5
  35.2 1.5 convolution_convert_fusion.6
  36.7 0.8 convert_element_type.106
  37.5 0.7 convert_element_type.107
  38.2 0.7 exp.26
  39.0 12.7 %reshape.106 = f32[7,64,64,64]{3,2,1,0:T(8,128)} reshape(f32[7,64,4096]{2,1,0:T(8,128)} %param.24) | data formatting | bytes 14680064 | tf_op jit(solution)/shard_map/reshape | solution.py:38
  51.7 1.5 convolution_convert_fusion.2
  53.3 0.7 all_to_all.48
  54.2 0.2 select_reduce_fusion
  54.7 0.2 multiply_exponential_fusion
  55.0 0.2 slice_reduce_fusion
  55.2 6.0 %all-to-all-start.1 = ((bf16[16,7,256]{2,1,0:T(8,128)(2,1)}), bf16[16,7,256]{2,1,0:T(8,128)(2,1)S(1)}, u32[]{:S(2)}, u32[]{:S(2)}) async-start(bf16[16,7,256]{2,1,0:T(8,128)(2,1)} %all_to_all.48), calls=%async_computation.1 | async-start | bytes 131072 | tf_op jit(solution)/shard_map/all_to_all | solution.py:90
  61.7 6.4 %all-to-all-done.1 = bf16[16,7,256]{2,1,0:T(8,128)(2,1)S(1)} async-done(((bf16[16,7,256]{2,1,0:T(8,128)(2,1)}), bf16[16,7,256]{2,1,0:T(8,128)(2,1)S(1)}, u32[]{:S(2)}, u32[]{:S(2)}) %all-to-all-start.1) | async-done | bytes 57376 | tf_op jit(solution)/shard_map/all_to_all | solution.py:90
  68.3 0.1 broadcast_multiply_fusion.2
  68.5 26.7 %fusion = f32[7,64,1,64]{3,2,1,0:T(1,128)S(1)} fusion(f32[7,64,64,1]{2,3,1,0:T(1,128)S(1)} %bitcast.68, f32[7,64,64,64]{3,2,1,0:T(8,128)} %reshape.106, f32[7,64]{1,0:T(8,128)S(1)} %get-tuple-element.17, f32[7,64,64]{2,1,0:T(8,128)S(1)} %bitcast.65, f32[7,64,64]{2,1,0:T(8,128)S(1)} %broadcast_multiply_fusion.2), kind=kOutput, calls=%fused_computation | convolution fusion | flops 27525120 | bytes 7800576 | tf_op jit(solution)/shard_map/bhpn,bhn->bhp/dot_general | solution.py:43
  95.1 0.2 multiply_reduce_fusion.1
  95.6 20.7 %all-gather.1 = bf16[16,7,4096]{2,1,0:T(8,128)(2,1)S(1)} all-gather(bf16[1,7,4096]{2,1,0:T(8,128)(2,1)S(1)} %fusion.37), channel_id=1, replica_groups=mesh['grp'=2,'ep'=16] {'ep'}, dimensions={0}, use_global_device_ids=true | all-gather | bytes 974848 | tf_op jit(solution)/shard_map/all_gather | solution.py:108
  116.3 1.2 reshape.121
  117.6 1.9 %convolution_convert_fusion.4 = bf16[112,128]{1,0:T(8,128)(2,1)S(1)} fusion(bf16[112,4096]{1,0:T(8,128)(2,1)} %reshape.121, bf16[4096,128]{1,0:T(8,128)(2,1)} %param.41), kind=kOutput, calls=%fused_computation.26 | convolution fusion | flops 117454848 | bytes 1994752 | tf_op jit(solution)/shard_map/dot_general | solution.py:107
  119.5 0.6 all_to_all.50
  120.1 3.5 %all-to-all-start.2 = ((bf16[16,7,128]{2,1,0:T(8,128)(2,1)}), bf16[16,7,128]{2,1,0:T(8,128)(2,1)S(1)}, u32[]{:S(2)}, u32[]{:S(2)}) async-start(bf16[16,7,128]{2,1,0:T(8,128)(2,1)} %all_to_all.50), calls=%async_computation.2 | async-start | bytes 65536 | tf_op jit(solution)/shard_map/all_to_all | solution.py:112
  123.6 8.7 %broadcast_multiply_fusion = f32[7,64,64,64]{3,2,1,0:T(8,128)} fusion(f32[7,64,64]{2,1,0:T(8,128)} %bitcast.66, f32[7,64,64]{2,1,0:T(8,128)S(1)} %broadcast_multiply_fusion.2), kind=kLoop, calls=%fused_computation.4 | loop fusion | flops 1835008 | bytes 7569408 | tf_op jit(solution)/shard_map/mul | solution.py:41
  132.3 12.9 %mul.261 = f32[7,64,4096]{2,1,0:T(8,128)} reshape(f32[7,64,64,64]{3,2,1,0:T(8,128)} %broadcast_multiply_fusion) | data formatting | bytes 14680064 | tf_op jit(solution)/shard_map/mul | solution.py:41
  145.1 0.1 fusion.34
  145.3 0.3 convolution_convert_fusion.1
  145.6 0.8 reshape.112
  146.4 6.0 %all-to-all-start.3 = ((bf16[16,3,2048]{2,1,0:T(4,128)(2,1)}), bf16[16,3,2048]{2,1,0:T(4,128)(2,1)S(1)}, u32[]{:S(2)}, u32[]{:S(2)}) async-start(bf16[16,3,2048]{2,1,0:T(4,128)(2,1)} %reshape.112), calls=%async_computation.3 | async-start | bytes 524288 | tf_op jit(solution)/shard_map/all_to_all | solution.py:132
  152.4 10.6 %multiply_add_fusion = f32[7,64,4096]{2,1,0:T(8,128)} fusion(f32[7,64,4096]{2,1,0:T(8,128)} %mul.261, f32[7,64,4096]{2,1,0:T(8,128)} %param.24, f32[7,64]{1,0:T(8,128)S(1)} %get-tuple-element.17), kind=kLoop, calls=%fused_computation.3 | loop fusion | flops 3670016 | bytes 22021888 | tf_op jit(solution)/shard_map/add | solution.py:40
  162.9 0.2 reshape.113
  163.1 2.0 %fusion.12 = f32[48,512]{1,0:T(8,128)S(1)} fusion(bf16[48,2048]{1,0:T(8,128)(2,1)S(1)} %reshape.113, bf16[1,2048,512]{2,1,0:T(8,128)(2,1)} %param.43), kind=kOutput, calls=%fused_computation.20 | convolution fusion | flops 100663296 | bytes 2392064 | tf_op jit(solution)/shard_map/dot_general | solution.py:135
  165.2 2.5 %convolution_convert_fusion = bf16[48,2048]{1,0:T(8,128)(2,1)S(1)} fusion(bf16[1,512,2048]{2,1,0:T(8,128)(2,1)S(1)} %copy-done, bf16[48,2048]{1,0:T(8,128)(2,1)S(1)} %reshape.113, bf16[1,2048,512]{2,1,0:T(8,128)(2,1)} %param.44, f32[48,512]{1,0:T(8,128)S(1)} %fusion.12), kind=kOutput, calls=%fused_computation.6 | convolution fusion | flops 201572352 | bytes 4685824 | tf_op jit(solution)/shard_map/dot_general | solution.py:138
  167.7 0.8 reshape.114
  168.5 6.0 %all-to-all-start.4 = ((bf16[16,3,2048]{2,1,0:T(4,128)(2,1)}), bf16[16,3,2048]{2,1,0:T(4,128)(2,1)S(1)}, u32[]{:S(2)}, u32[]{:S(2)}) async-start(bf16[16,3,2048]{2,1,0:T(4,128)(2,1)} %reshape.114), calls=%async_computation.4 | async-start | bytes 524288 | tf_op jit(solution)/shard_map/all_to_all | solution.py:141
  174.5 0.7 fusion.24
  175.3 9.3 %all-to-all-done.4 = bf16[16,3,2048]{2,1,0:T(4,128)(2,1)S(1)} async-done(((bf16[16,3,2048]{2,1,0:T(4,128)(2,1)}), bf16[16,3,2048]{2,1,0:T(4,128)(2,1)S(1)}, u32[]{:S(2)}, u32[]{:S(2)}) %all-to-all-start.4) | async-done | bytes 196640 | tf_op jit(solution)/shard_map/all_to_all | solution.py:141
  184.5 0.2 reshape.115
  184.7 0.2 convolution_multiply_fusion.3
  184.9 0.2 fusion.7
  185.1 0.2 fusion.6
  185.3 0.8 fusion.8
  (59 shorter events, 1.5 us)
Async XLA Ops:
  0.6 164.5 %copy-start = (bf16[1,512,2048]{2,1,0:T(8,128)(2,1)S(1)}, bf16[1,512,2048]{2,1,0:T(8,128)(2,1)}, u32[]{:S(2)}) copy-start(bf16[1,512,2048]{2,1,0:T(8,128)(2,1)} %param.45) | copy-start | bytes 6291460
  30.2 25.0 %all-to-all-start = ((bf16[16,7,256]{2,1,0:T(8,128)(2,1)}), bf16[16,7,256]{2,1,0:T(8,128)(2,1)S(1)}, u32[]{:S(2)}, u32[]{:S(2)}) async-start(bf16[16,7,256]{2,1,0:T(8,128)(2,1)} %all_to_all.44), calls=%async_computation | async-start | bytes 131072 | tf_op jit(solution)/shard_map/all_to_all | solution.py:93
  38.9 15.0 %copy-start.5 = (bf16[4096]{0:T(1024)(128)(2,1)S(1)}, bf16[4096]{0:T(1024)(128)(2,1)}, u32[]{:S(2)}) copy-start(bf16[4096]{0:T(1024)(128)(2,1)} %param.40) | copy-start | bytes 24580
  38.9 15.0 %copy-start.8 = (s32[7,4]{0,1:T(4,128)S(1)}, s32[7,4]{0,1:T(4,128)}, u32[]{:S(2)}) copy-start(s32[7,4]{0,1:T(4,128)} %param.26) | copy-start | bytes 340
  38.9 15.7 %copy-start.7 = (bf16[2048]{0:T(1024)(128)(2,1)S(1)}, bf16[2048]{0:T(1024)(128)(2,1)}, u32[]{:S(2)}) copy-start(bf16[2048]{0:T(1024)(128)(2,1)} %param.42) | copy-start | bytes 12292
  38.9 15.7 %copy-start.6 = (f32[7,4]{0,1:T(4,128)S(1)}, f32[7,4]{0,1:T(4,128)}, u32[]{:S(2)}) copy-start(f32[7,4]{0,1:T(4,128)} %param.28) | copy-start | bytes 340
  38.9 15.7 %copy-start.10 = (f32[7]{0:T(128)S(1)}, f32[7]{0:T(128)}, u32[]{:S(2)}) copy-start(f32[7]{0:T(128)} %param.27) | copy-start | bytes 88
  38.9 15.8 %copy-start.2 = (bf16[7,2048]{1,0:T(8,128)(2,1)S(1)}, bf16[7,2048]{1,0:T(8,128)(2,1)}, u32[]{:S(2)}) copy-start(bf16[7,2048]{1,0:T(8,128)(2,1)} %param.23) | copy-start | bytes 86020
  38.9 15.8 %copy-start.11 = (bf16[2048,64]{0,1:T(8,128)(2,1)S(1)}, bf16[2048,64]{0,1:T(8,128)(2,1)}, u32[]{:S(2)}) copy-start(bf16[2048,64]{0,1:T(8,128)(2,1)} %param.34) | copy-start | bytes 786436
  39.0 15.8 %copy-start.12 = (f32[64]{0:T(128)S(1)}, f32[64]{0:T(128)}, u32[]{:S(2)}) copy-start(f32[64]{0:T(128)} %param.37) | copy-start | bytes 772
  39.0 22.3 %copy-start.3 = (bf16[7,3,4608]{2,0,1:T(8,128)(2,1)S(1)}, bf16[7,3,4608]{2,0,1:T(8,128)(2,1)}, u32[]{:S(2)}) copy-start(bf16[7,3,4608]{2,0,1:T(8,128)(2,1)} %param.25) | copy-start | bytes 580612
  55.2 12.9 %all-to-all-start.1 = ((bf16[16,7,256]{2,1,0:T(8,128)(2,1)}), bf16[16,7,256]{2,1,0:T(8,128)(2,1)S(1)}, u32[]{:S(2)}, u32[]{:S(2)}) async-start(bf16[16,7,256]{2,1,0:T(8,128)(2,1)} %all_to_all.48), calls=%async_computation.1 | async-start | bytes 131072 | tf_op jit(solution)/shard_map/all_to_all | solution.py:90
  68.4 26.7 %copy-start.1 = (f32[7,4,16,64]{3,2,1,0:T(8,128)}, f32[7,4,16,64]{3,2,1,0:T(8,128)S(1)}, u32[]{:S(2)}) copy-start(f32[7,4,16,64]{3,2,1,0:T(8,128)S(1)} %broadcast_in_dim.7) | copy-start | bytes 344068
  68.5 26.7 %copy-start.9 = (f32[64]{0:T(128)S(1)}, f32[64]{0:T(128)}, u32[]{:S(2)}) copy-start(f32[64]{0:T(128)} %param.39) | copy-start | bytes 772
  120.1 25.1 %all-to-all-start.2 = ((bf16[16,7,128]{2,1,0:T(8,128)(2,1)}), bf16[16,7,128]{2,1,0:T(8,128)(2,1)S(1)}, u32[]{:S(2)}, u32[]{:S(2)}) async-start(bf16[16,7,128]{2,1,0:T(8,128)(2,1)} %all_to_all.50), calls=%async_computation.2 | async-start | bytes 65536 | tf_op jit(solution)/shard_map/all_to_all | solution.py:112
  146.4 16.6 %all-to-all-start.3 = ((bf16[16,3,2048]{2,1,0:T(4,128)(2,1)}), bf16[16,3,2048]{2,1,0:T(4,128)(2,1)S(1)}, u32[]{:S(2)}, u32[]{:S(2)}) async-start(bf16[16,3,2048]{2,1,0:T(4,128)(2,1)} %reshape.112), calls=%async_computation.3 | async-start | bytes 524288 | tf_op jit(solution)/shard_map/all_to_all | solution.py:132
  162.9 11.6 %copy-start.4 = (bf16[7,3,4608]{2,0,1:T(8,128)(2,1)S(1)}, bf16[7,3,4608]{2,0,1:T(8,128)(2,1)}, u32[]{:S(2)}) copy-start(bf16[7,3,4608]{2,0,1:T(8,128)(2,1)} %param.25) | copy-start | bytes 580612
  168.5 16.0 %all-to-all-start.4 = ((bf16[16,3,2048]{2,1,0:T(4,128)(2,1)}), bf16[16,3,2048]{2,1,0:T(4,128)(2,1)S(1)}, u32[]{:S(2)}, u32[]{:S(2)}) async-start(bf16[16,3,2048]{2,1,0:T(4,128)(2,1)} %reshape.114), calls=%async_computation.4 | async-start | bytes 524288 | tf_op jit(solution)/shard_map/all_to_all | solution.py:141
where the time goes:
time: 188 us; the launch traced here: 186 us
  blocking collectives  45.3 us (24%)
  matrix products  41.2 us (22%)
  local copies, waits for them, and re-layouts  32.7 us (17%)
  other arithmetic  25.3 us (13%)
  starting transfers between devices  25 us (13%)
  waiting for transfers between devices  15.7 us (8%)
    dot_general x1, matrix products, state_step(): jnp.einsum('bhpn,bhn->bhp', carried, c_heads, precision=lax.Precision.HIG...  26.7 us
    all_gather x1, blocking collectives, body(): row_part = lax.all_gather(normed, 'ep', axis=0, tiled=True)  24.6 us
    all_gather x1, blocking collectives, body(): lax.all_gather(y_mix, 'ep', axis=0, tiled=True)  20.7 us
    mul x1, local copies, waits for them, and re-layouts, state_step(): (step_size[:, :, None] * x_heads)[:, :, :, None] * b_heads[:, :, None, :]  12.9 us
    reshape x1, local copies, waits for them, and re-layouts, state_step(): carried = state_in.reshape(row_count, HEADS, HEAD_DIM, STATE)  12.7 us
    add x1, other arithmetic, state_step(): decay_rate[:, :, None, None] * carried  10.6 us
    all_to_all x1, waiting for transfers between devices, body(): lax.all_to_all(expert_out.reshape(sources, slots_here, width), 'ep', spli...  9.27 us
    mul x1, other arithmetic, state_step(): (step_size[:, :, None] * x_heads)[:, :, :, None] * b_heads[:, :, None, :]  8.67 us
  transfers between devices with their start and end apart: 5, of which 2 were waited for; matrix products, arithmetic and copies ran while one was open for 29% of the time, Pallas kernels for 0%

commit v1 on v0

v1 whole, which is shorter than its diff:
```python
import functools

import jax
import jax.numpy as jnp
from jax import lax
from jax.experimental import pallas as pl
from jax.experimental.pallas import tpu as pltpu
from jax.sharding import PartitionSpec as P

HEADS = 64
HEAD_DIM = 64
SSM_GROUPS = 4
STATE = 64
TOP = 4
EPS = 1e-06
MESH = pl.DeviceIdType.MESH
F32 = jnp.float32
BF16 = jnp.bfloat16
ROWS = 8


def rms_scale(values, gain_vec):
    return (
        values
        * lax.rsqrt(jnp.mean(values * values, axis=-1, keepdims=True) + EPS)
        * gain_vec.astype(F32)
    )


def peer(index):
    return (lax.axis_index("grp"), index)


def enter(n):
    me = lax.axis_index("ep")
    barrier = pltpu.get_barrier_semaphore()

    for d in range(1, n):
        pl.semaphore_signal(
            barrier, inc=1, device_id=peer(lax.rem(me + d, n)), device_id_type=MESH
        )
    pl.semaphore_wait(barrier, n - 1)


def remote(src, dst, send_sem, recv_sem, index):
    return pltpu.make_async_remote_copy(
        src_ref=src,
        dst_ref=dst,
        send_sem=send_sem,
        recv_sem=recv_sem,
        device_id=peer(index),
        device_id_type=MESH,
    )


def gather_start(n, src, buf, send, recv):
    me = lax.axis_index("ep")
    copies = []
    for d in range(1, n // 4):
        copy = remote(src, buf.at[me], send.at[d - 1], recv.at[d - 1], lax.rem(me + 4 * d, n))
        copy.start()
        copies.append(copy)
    return copies


def gather_finish(n, src, buf, send, recv, copies):
    me = lax.axis_index("ep")
    outer = n // 4
    core = lax.rem(me, 2)
    mid = lax.rem(me // 2, 2)
    mate = me + 1 - 2 * core
    across = me + 2 - 4 * mid
    second, third, fourth = [], [], []
    base = outer - 1
    for d in range(outer):
        block = lax.rem(me + n - 4 * d, n)
        if d > 0:
            copies[d - 1].wait_recv()
        piece = src if d == 0 else buf.at[block]
        copy = remote(piece, buf.at[block], send.at[base + d], recv.at[base + d], across)
        copy.start()
        second.append(copy)
        copy = remote(
            piece, buf.at[block], send.at[base + outer + d], recv.at[base + outer + d], mate
        )
        copy.start()
        third.append(copy)
    for d in range(outer):
        block = lax.rem(across + n - 4 * d, n)
        second[d].wait_recv()
        slot = base + 2 * outer + d
        copy = remote(buf.at[block], buf.at[block], send.at[slot], recv.at[slot], mate)
        copy.start()
        fourth.append(copy)
    for copy in third + fourth:
        copy.wait_recv()
    for copy in copies + second + third + fourth:
        copy.wait_send()


def exchange(n, out_buf, in_buf, send, recv):
    me = lax.axis_index("ep")
    copies = []
    for d in range(1, n):
        to = lax.rem(me + d, n)
        copy = remote(out_buf.at[to], in_buf.at[me], send.at[d - 1], recv.at[d - 1], to)
        copy.start()
        copies.append(copy)
    in_buf[me] = out_buf[me]
    for copy in copies:
        copy.wait_recv()
    for copy in copies:
        copy.wait_send()


def project_kernel(
    n,
    hid_ref,
    gain_ref,
    z_any,
    x_any,
    b_any,
    c_any,
    dt_any,
    all_ref,
    z_ref,
    x_ref,
    bc_ref,
    dt_ref,
    hbuf,
    normed,
    zw,
    xw,
    bw,
    cw,
    dw,
    out_buf,
    in_buf,
    wsem,
    gs,
    gr,
    es,
    er,
):
    loads = [
        pltpu.make_async_copy(src, dst, wsem.at[i])
        for i, (src, dst) in enumerate(
            [(b_any, bw), (c_any, cw), (dt_any, dw), (z_any, zw), (x_any, xw)]
        )
    ]
    for load in loads:
        load.start()
    enter(n)
    me = lax.axis_index("ep")
    copies = gather_start(n, hid_ref, hbuf, gs, gr)
    hbuf[me] = hid_ref[...]
    gain = gain_ref[...]
    mine = rms_scale(hid_ref[...].astype(F32), gain).astype(BF16)
    for load in loads[:3]:
        load.wait()
    span = bw.shape[1]
    bc_ref[:, :span] = jnp.dot(mine, bw[...], preferred_element_type=F32).astype(BF16).astype(F32)
    bc_ref[:, span:] = jnp.dot(mine, cw[...], preferred_element_type=F32).astype(BF16).astype(F32)
    dt_ref[...] = jnp.dot(mine, dw[...], preferred_element_type=F32).astype(BF16).astype(F32)
    gather_finish(n, hid_ref, hbuf, gs, gr, copies)
    for j in range(0, n, 2):
        pair = jnp.concatenate([hbuf[j].astype(F32), hbuf[j + 1].astype(F32)], axis=0)
        all_ref[j * ROWS : (j + 2) * ROWS, :] = pair.astype(BF16)
        normed[j * ROWS : (j + 2) * ROWS, :] = rms_scale(pair, gain).astype(BF16)
    for load in loads[3:]:
        load.wait()
    cols = zw.shape[1]
    z_part = jnp.dot(normed[...], zw[...], preferred_element_type=F32)
    x_part = jnp.dot(normed[...], xw[...], preferred_element_type=F32)
    for j in range(n):
        out_buf[j, :, :cols] = z_part[j * ROWS : (j + 1) * ROWS].astype(BF16)
        out_buf[j, :, cols:] = x_part[j * ROWS : (j + 1) * ROWS].astype(BF16)
    exchange(n, out_buf, in_buf, es, er)
    for j in range(n):
        z_ref[:, j * cols : (j + 1) * cols] = in_buf[j, :, :cols].astype(F32)
        x_ref[:, j * cols : (j + 1) * cols] = in_buf[j, :, cols:].astype(F32)


def project(n, hid8, first_gain, z_weight, x_weight, b_weight, c_weight, dt_weight):
    width = hid8.shape[1]
    cols = z_weight.shape[1]
    inner = n * cols
    span = b_weight.shape[1]
    vm = pl.BlockSpec(memory_space=pltpu.VMEM)
    hbm = pl.BlockSpec(memory_space=pl.ANY)
    dma = pltpu.SemaphoreType.DMA
    return pl.pallas_call(
        functools.partial(project_kernel, n),
        out_shape=(
            jax.ShapeDtypeStruct((n * ROWS, width), BF16),
            jax.ShapeDtypeStruct((ROWS, inner), F32),
            jax.ShapeDtypeStruct((ROWS, inner), F32),
            jax.ShapeDtypeStruct((ROWS, 2 * span), F32),
            jax.ShapeDtypeStruct((ROWS, dt_weight.shape[1]), F32),
        ),
        in_specs=[vm, vm] + [hbm] * 5,
        out_specs=(vm,) * 5,
        scratch_shapes=[
            pltpu.VMEM((n, ROWS, width), BF16),
            pltpu.VMEM((n * ROWS, width), BF16),
            pltpu.VMEM(z_weight.shape, BF16),
            pltpu.VMEM(x_weight.shape, BF16),
            pltpu.VMEM(b_weight.shape, BF16),
            pltpu.VMEM(c_weight.shape, BF16),
            pltpu.VMEM(dt_weight.shape, BF16),
            pltpu.VMEM((n, ROWS, 2 * cols), BF16),
            pltpu.VMEM((n, ROWS, 2 * cols), BF16),
            dma((5,)),
            dma((n - 1,)),
            dma((n - 1,)),
            dma((n - 1,)),
            dma((n - 1,)),
        ],
        compiler_params=pltpu.CompilerParams(
            collective_id=0, has_side_effects=True, vmem_limit_bytes=40 << 20
        ),
        name="project",
    )(hid8, first_gain[None, :], z_weight, x_weight, b_weight, c_weight, dt_weight)


def state_kernel(heads_ref, bc_ref, par_ref, gain_ref, st_ref, out_ref, y_ref):
    s = pl.program_id(0)
    heads = heads_ref[0]
    x = heads[:, :HEAD_DIM]
    z = heads[:, HEAD_DIM : 2 * HEAD_DIM]
    dt = heads[:, 2 * HEAD_DIM : 2 * HEAD_DIM + 1]
    par = par_ref[...]
    step = jax.nn.softplus(dt + par[:, 0:1])
    decay = jnp.exp(-step * jnp.exp(par[:, 1:2]))
    sx = step * x
    sx = jnp.concatenate([sx, sx], axis=1)
    row = bc_ref[pl.ds(s, 1), :]
    span = SSM_GROUPS * STATE
    per = HEADS // SSM_GROUPS
    bs, cs = [], []
    for g in range(SSM_GROUPS):
        b = row[:, g * STATE : (g + 1) * STATE]
        c = row[:, span + g * STATE : span + (g + 1) * STATE]
        bs.append(jnp.broadcast_to(jnp.concatenate([b, b], axis=1), (per, 2 * STATE)))
        cs.append(jnp.broadcast_to(jnp.concatenate([c, c], axis=1), (per, 2 * STATE)))
    b_all = jnp.concatenate(bs, axis=0)
    c_all = jnp.concatenate(cs, axis=0)
    decay = jnp.broadcast_to(decay, (HEADS, 128))
    half = lax.broadcasted_iota(jnp.int32, (HEADS, 128), 1) // STATE
    blocks = HEAD_DIM * STATE // 256
    k_of = lax.broadcasted_iota(jnp.int32, (256, 128), 0) // STATE
    l_of = lax.broadcasted_iota(jnp.int32, (256, 128), 1)
    fold = (k_of == l_of).astype(F32).astype(BF16)
    prods = []
    for k in range(blocks):
        parts = []
        for i in range(2):
            lane = (2 * k + i) * 128
            grown = jnp.take_along_axis(sx, half + (4 * k + 2 * i), axis=1)
            new = decay * st_ref[0, :, lane : lane + 128] + grown * b_all
            out_ref[0, :, lane : lane + 128] = new
            parts.append((new * c_all).astype(BF16))
        prods.append(jnp.concatenate(parts, axis=1))
    sums = jnp.dot(jnp.concatenate(prods, axis=0), fold, preferred_element_type=F32)
    total = sums[:HEADS]
    for k in range(1, blocks):
        total = total + pltpu.roll(sums[k * HEADS : (k + 1) * HEADS], 4 * k, 1)
    readout = total[:, :HEAD_DIM] + par[:, 2:3] * x
    gated = readout * jax.nn.silu(z)
    mean = jnp.sum(gated * gated, keepdims=True) / (HEADS * HEAD_DIM)
    y_ref[0] = gated * lax.rsqrt(mean + EPS) * gain_ref[...]


def state_update(heads, bc, par, gain, state_in):
    rows, _, flat = state_in.shape
    return pl.pallas_call(
        state_kernel,
        grid=(rows,),
        out_shape=(
            jax.ShapeDtypeStruct(state_in.shape, F32),
            jax.ShapeDtypeStruct((rows, HEADS, HEAD_DIM), F32),
        ),
        in_specs=[
            pl.BlockSpec((1,) + heads.shape[1:], lambda s: (s, 0, 0)),
            pl.BlockSpec(bc.shape, lambda s: (0, 0)),
            pl.BlockSpec(par.shape, lambda s: (0, 0)),
            pl.BlockSpec(gain.shape, lambda s: (0, 0)),
            pl.BlockSpec((1, HEADS, flat), lambda s: (s, 0, 0)),
        ],
        out_specs=(
            pl.BlockSpec((1, HEADS, flat), lambda s: (s, 0, 0)),
            pl.BlockSpec((1, HEADS, HEAD_DIM), lambda s: (s, 0, 0)),
        ),
        compiler_params=pltpu.CompilerParams(vmem_limit_bytes=40 << 20),
        name="state",
    )(heads, bc, par, gain, state_in)


def expert_kernel(
    n,
    cap,
    y_ref,
    hid_ref,
    own_ref,
    ids_ref,
    prob_ref,
    score_ref,
    gain_ref,
    ow_any,
    eg_any,
    eu_any,
    ed_any,
    out_ref,
    ybuf,
    yflat,
    pbuf,
    mixed,
    normed,
    act,
    eo,
    ow,
    eg,
    eu,
    ed,
    out_buf,
    in_buf,
    wsem,
    ys,
    yr,
    ps,
    pr,
    es,
    er,
):
    loads = [
        pltpu.make_async_copy(src, dst, wsem.at[i])
        for i, (src, dst) in enumerate(
            [(ow_any, ow), (eg_any.at[0], eg), (eu_any.at[0], eu), (ed_any.at[0], ed)]
        )
    ]
    for load in loads:
        load.start()
    enter(n)
    me = lax.axis_index("ep")
    total = n * ROWS
    copies = gather_start(n, y_ref, ybuf, ys, yr)
    ybuf[me] = y_ref[...]
    q = lax.broadcasted_iota(jnp.int32, (total, total), 0)
    t = lax.broadcasted_iota(jnp.int32, (total, total), 1)
    last = (t == (q // ROWS) * ROWS + (ROWS - 1)).astype(F32).astype(BF16)
    ids = jnp.dot(last, hid_ref[:, :128], preferred_element_type=F32)
    flags = (ids == me.astype(F32)).astype(F32).astype(BF16)
    lane = lax.broadcasted_iota(jnp.int32, (128, total), 0) // TOP
    token = lax.rem(lax.broadcasted_iota(jnp.int32, (128, total), 1), ROWS)
    here = jnp.dot(flags, (lane == token).astype(F32).astype(BF16), preferred_element_type=F32)
    before = jnp.dot(flags, (lane < token).astype(F32).astype(BF16), preferred_element_type=F32)
    slot = lax.rem(q, ROWS).astype(F32)
    chosen = (q // ROWS == t // ROWS) & (here > 0.5) & (before == slot)
    select = chosen.astype(F32).astype(BF16)
    rows = out_ref.shape[0]
    col = lax.broadcasted_iota(jnp.int32, (rows, n * cap), 1)
    score = score_ref[...]
    share = prob_ref[...] * score / jnp.sum(score, axis=1, keepdims=True)
    weight = jnp.zeros((rows, n * cap), F32)
    used = jnp.zeros((rows, n * cap), F32)
    for pick in range(TOP):
        hit = (ids_ref[:, pick : pick + 1] == col // cap).astype(F32)
        used = used + hit
        weight = weight + hit * share[:, pick : pick + 1]
    row_id = lax.broadcasted_iota(jnp.int32, (rows, n * cap), 0)
    rank = jnp.zeros((rows, n * cap), F32)
    for r in range(rows - 1):
        rank = rank + jnp.where(row_id > r, used[r : r + 1, :], 0.0)
    weight = jnp.where(rank == lax.rem(col, cap).astype(F32), weight, 0.0)
    high = weight.astype(BF16)
    low = (weight - high.astype(F32)).astype(BF16)
    gather_finish(n, y_ref, ybuf, ys, yr, copies)
    for j in range(0, n, 2):
        pair = jnp.concatenate([ybuf[j].astype(F32), ybuf[j + 1].astype(F32)], axis=0)
        yflat[j * ROWS : (j + 2) * ROWS, :] = pair.astype(BF16)
    loads[0].wait()
    pbuf[me] = jnp.dot(yflat[...], ow[...], preferred_element_type=F32).astype(BF16)
    copies = gather_start(n, pbuf.at[me], pbuf, ps, pr)
    gather_finish(n, pbuf.at[me], pbuf, ps, pr, copies)
    cols = pbuf.shape[2]
    for j in range(n):
        at = slice(j * cols, (j + 1) * cols)
        mixed[:, at] = (hid_ref[:, at].astype(F32) + pbuf[j].astype(F32)).astype(BF16)
    for j in range(0, total, 16):
        normed[j : j + 16, :] = rms_scale(mixed[j : j + 16, :].astype(F32), gain_ref[...]).astype(
            BF16
        )
    for load in loads[1:]:
        load.wait()
    for j in range(0, eg.shape[1], 256):
        at = slice(j, j + 256)
        gate = jnp.dot(normed[...], eg[:, at], preferred_element_type=F32)
        up = jnp.dot(normed[...], eu[:, at], preferred_element_type=F32)
        act[:, at] = (jax.nn.silu(gate) * up).astype(BF16)
    width = eo.shape[1]

    def down(i, carry):
        at = pl.ds(pl.multiple_of(i * 256, 256), 256)
        part = jnp.dot(act[...], ed[:, at], preferred_element_type=F32).astype(BF16)
        eo[:, at] = jnp.dot(select, part, preferred_element_type=F32)
        return carry

    lax.fori_loop(0, width // 256, down, 0)
    for j in range(n):
        out_buf[j] = eo[j * ROWS : j * ROWS + cap, :].astype(BF16)
    exchange(n, out_buf, in_buf, es, er)
    per = ROWS // cap
    for j in range(0, n, per):
        eo[j * cap : (j + per) * cap, :] = jnp.concatenate(
            [in_buf[j + i].astype(F32) for i in range(per)], axis=0
        )
    back = eo[: n * cap, :].astype(BF16)
    moe = jnp.dot(high, back, preferred_element_type=F32) + jnp.dot(
        low, back, preferred_element_type=F32
    )
    start = pl.multiple_of(me * ROWS, ROWS)
    eo[...] = mixed[...].astype(F32)
    out_ref[...] = (eo[pl.ds(start, ROWS), :][:rows] + moe).astype(BF16)


def experts(
    n, cap, y8, hid_all, hidden, ids, prob, score, second_gain, out_weight, gate_w, up_w, down_w
):
    total, width = hid_all.shape
    inner = y8.shape[1]
    cols = out_weight.shape[1]
    hid_units = gate_w.shape[2]
    vm = pl.BlockSpec(memory_space=pltpu.VMEM)
    hbm = pl.BlockSpec(memory_space=pl.ANY)
    dma = pltpu.SemaphoreType.DMA
    return pl.pallas_call(
        functools.partial(expert_kernel, n, cap),
        out_shape=jax.ShapeDtypeStruct(hidden.shape, BF16),
        in_specs=[vm] * 7 + [hbm] * 4,
        out_specs=vm,
        scratch_shapes=[
            pltpu.VMEM((n, ROWS, inner), BF16),
            pltpu.VMEM((total, inner), BF16),
            pltpu.VMEM((n, total, cols), BF16),
            pltpu.VMEM((total, width), BF16),
            pltpu.VMEM((total, width), BF16),
            pltpu.VMEM((total, hid_units), BF16),
            pltpu.VMEM((total, width), F32),
            pltpu.VMEM(out_weight.shape, BF16),
            pltpu.VMEM(gate_w.shape[1:], BF16),
            pltpu.VMEM(up_w.shape[1:], BF16),
            pltpu.VMEM(down_w.shape[1:], BF16),
            pltpu.VMEM((n, cap, width), BF16),
            pltpu.VMEM((n, cap, width), BF16),
            dma((4,)),
        ]
        + [dma((n - 1,))] * 6,
        compiler_params=pltpu.CompilerParams(
            collective_id=1, has_side_effects=True, vmem_limit_bytes=48 << 20
        ),
        name="experts",
    )(
        y8,
        hid_all,
        hidden,
        ids,
        prob[:, None],
        score,
        second_gain[None, :],
        out_weight,
        gate_w,
        up_w,
        down_w,
    )


def body(
    hidden,
    state_in,
    conv_state,
    expert_ids,
    group_prob,
    expert_score,
    first_gain,
    z_weight,
    x_weight,
    b_weight,
    c_weight,
    dt_weight,
    conv_weight,
    conv_bias,
    dt_bias,
    decay_log,
    skip_gain,
    inner_gain,
    out_weight,
    second_gain,
    expert_gate,
    expert_up,
    expert_down,
):
    n = lax.axis_size("ep")
    rows, width = hidden.shape
    inner = HEADS * HEAD_DIM
    id_row = jnp.pad(
        expert_ids.astype(BF16).reshape(1, -1),
        ((0, 0), (0, width - rows * TOP)),
        constant_values=-1,
    )
    hid8 = jnp.concatenate([hidden, id_row], axis=0)
    hid_all, z8, x8, bc8, dt8 = project(
        n, hid8, first_gain, z_weight, x_weight, b_weight, c_weight, dt_weight
    )
    fresh = jnp.concatenate([x8[:rows], bc8[:rows]], axis=1).astype(BF16)
    window = jnp.concatenate([conv_state, fresh[:, None, :]], axis=1)
    summed = jnp.sum(window.astype(F32) * conv_weight.astype(F32)[None], axis=1)
    active = jax.nn.silu(summed + conv_bias.astype(F32)[None, :])
    heads = jnp.concatenate(
        [
            active[:, :inner].reshape(rows, HEADS, HEAD_DIM),
            z8[:rows].reshape(rows, HEADS, HEAD_DIM),
            dt8[:rows][:, :, None],
        ],
        axis=2,
    )
    par = jnp.stack([dt_bias, decay_log, skip_gain], axis=1)
    state_out, y_heads = state_update(
        heads,
        active[:, inner:],
        par,
        inner_gain.astype(F32).reshape(HEADS, HEAD_DIM),
        state_in,
    )
    y8 = jnp.pad(y_heads.astype(BF16).reshape(rows, inner), ((0, ROWS - rows), (0, 0)))
    need = max(2, (3 * rows * TOP + 2 * n - 1) // (2 * n))
    cap = 2 if need <= 2 else 4 if need <= 4 else 8
    layer_out = experts(
        n,
        cap,
        y8,
        hid_all,
        hidden,
        expert_ids,
        group_prob,
        expert_score,
        second_gain,
        out_weight,
        expert_gate,
        expert_up,
        expert_down,
    )
    return (layer_out, state_out, window[:, 1:, :])


def solution(mesh):
    in_specs = (
        P(("grp", "ep"), None),
        P(("grp", "ep"), None, None),
        P(("grp", "ep"), None, None),
        P(("grp", "ep"), None),
        P(("grp", "ep")),
        P(("grp", "ep"), None),
        P(),
        P(None, "ep"),
        P(None, "ep"),
        P(),
        P(),
        P(),
        P(),
        P(),
        P(),
        P(),
        P(),
        P(),
        P(None, "ep"),
        P(),
        P("ep", None, None),
        P("ep", None, None),
        P("ep", None, None),
    )
    out_specs = (P(("grp", "ep"), None), P(("grp", "ep"), None, None), P(("grp", "ep"), None, None))
    return jax.shard_map(body, mesh=mesh, in_specs=in_specs, out_specs=out_specs, check_vma=False)
```

time: 188 us -> 83.8 us (0.45)
  Pallas kernels: 0 us -> 65.1 us
  blocking collectives: 45.3 us -> 0 us
  matrix products: 41.2 us -> 0 us
  starting transfers between devices: 25 us -> 0 us
  other arithmetic: 25.3 us -> 1.9 us
  local copies, waits for them, and re-layouts: 32.7 us -> 15.3 us
  waiting for transfers between devices: 15.7 us -> 0 us
    pallas_call x0 -> x3, Pallas kernels: none -> 65.1 us  [the longest x1 36.4 us: experts(): pl.pallas_call(functools.partial(expert_kernel, n, cap), out_shape=jax.Sh...]
    all_gather x2 -> x0, blocking collectives: 45.3 us -> none  [the longest x1 24.6 us: body(): row_part = lax.all_gather(normed, 'ep', axis=0, tiled=True)]
    dot_general x14 -> x0, matrix products: 41.2 us -> none  [the longest x1 26.7 us: state_step(): jnp.einsum('bhpn,bhn->bhp', carried, c_heads, precision=lax.Precision.HIG...]
    all_to_all x5 -> x0, starting transfers between devices: 25 us -> none  [the longest x1 6 us: body(): lax.all_to_all(expert_out.reshape(sources, slots_here, width), 'ep', spli...]
    all_to_all x5 -> x0, waiting for transfers between devices: 15.7 us -> none  [the longest x1 9.27 us: body(): lax.all_to_all(expert_out.reshape(sources, slots_here, width), 'ep', spli...]
    reshape x9 -> x5, local copies, waits for them, and re-layouts: 15.1 us -> 0.5 us  [the longest x1 0.14 us: body(): y_heads.astype(BF16).reshape(rows, inner)]
    mul x2 -> x0, local copies, waits for them, and re-layouts: 12.9 us -> none  [the longest x1 12.9 us: state_step(): (step_size[:, :, None] * x_heads)[:, :, :, None] * b_heads[:, :, None, :]]
    unnamed x29 -> x44, local copies, waits for them, and re-layouts: 1.58 us -> 12.9 us
  transfers between devices with their start and end apart: 5 -> 0, of which waited for: 2 -> 0; matrix products, arithmetic and copies ran while one was open for 29% -> 0% of each run, Pallas kernels for 0% -> 0%
where the time goes in v1:
time: 83.8 us; the launch traced here: 83.2 us
  Pallas kernels  65.1 us (78%)
  local copies, waits for them, and re-layouts  15.3 us (18%)
  other arithmetic  1.9 us (2%)
  between operations  0.9 us (1%)
    pallas_call x1, Pallas kernels, experts(): pl.pallas_call(functools.partial(expert_kernel, n, cap), out_shape=jax.Sh...  36.4 us
    pallas_call x1, Pallas kernels, project(): pl.pallas_call(functools.partial(project_kernel, n), out_shape=(jax.Shape...  20.6 us
    unnamed x44, local copies, waits for them, and re-layouts  12.9 us
    pallas_call x1, Pallas kernels, state_update(): pl.pallas_call(state_kernel, grid=(rows,), out_shape=(jax.ShapeDtypeStruc...  8.06 us

profile of v1, /device:TPU:0, one launch (start us, length us, event | category | flops | bytes accessed | tf_op | source)
XLA Modules:
  0.0 83.2 jit_solution(14366170572959350228)
XLA Ops:
  0.6 1.2 %copy.44.dt_any = bf16[2048,64]{1,0:T(8,128)(2,1)S(1)} copy(bf16[2048,64]{0,1:T(8,128)(2,1)} %param.34) | data formatting | bytes 524288 | tf_op args[11]
  1.9 0.7 convert_element_type.28
  2.5 0.1 copy.43
  2.7 0.1 reshape.56
  2.7 0.8 fusion.2.hid_ref
  3.5 0.7 broadcast_in_dim.15.gain_ref
  4.2 1.2 %copy-done.4 = bf16[2048,256]{1,0:T(8,128)(2,1)S(1)} copy-done((bf16[2048,256]{1,0:T(8,128)(2,1)S(1)}, bf16[2048,256]{1,0:T(8,128)(2,1)}, u32[]{:S(2)}) %copy-start.4) | copy-done | bytes 1048600
  5.4 1.2 %copy-done.5 = bf16[2048,256]{1,0:T(8,128)(2,1)S(1)} copy-done((bf16[2048,256]{1,0:T(8,128)(2,1)S(1)}, bf16[2048,256]{1,0:T(8,128)(2,1)}, u32[]{:S(2)}) %copy-start.5) | copy-done | bytes 1048600
  6.7 1.2 %copy-done.6 = bf16[2048,256]{1,0:T(8,128)(2,1)S(1)} copy-done((bf16[2048,256]{1,0:T(8,128)(2,1)S(1)}, bf16[2048,256]{1,0:T(8,128)(2,1)}, u32[]{:S(2)}) %copy-start.6) | copy-done | bytes 1048600
  7.9 1.2 %copy-done.7 = bf16[2048,256]{1,0:T(8,128)(2,1)S(1)} copy-done((bf16[2048,256]{1,0:T(8,128)(2,1)S(1)}, bf16[2048,256]{1,0:T(8,128)(2,1)}, u32[]{:S(2)}) %copy-start.7) | copy-done | bytes 1048600
  9.1 20.6 %project.1 = (bf16[128,2048]{1,0:T(8,128)(2,1)S(1)}, f32[8,4096]{1,0:T(8,128)S(1)}, f32[8,4096]{1,0:T(8,128)S(1)}, f32[8,512]{1,0:T(8,128)S(1)}, f32[8,64]{1,0:T(8,128)S(1)}) custom-call(bf16[8,2048]{1,0:T(8,128)(2,1)S(1)} %fusion.2.hid_ref, bf16[1,2048]{1,0:T(2,128)(2,1)S(1)} %broadcast_in_dim.15.gain_ref, bf16[2048,256]{1,0:T(8,128)(2,1)S(1)} %copy-done.4, ...), custom_call_target="tpu_custom_call" | custom-call | tf_op jit(solution)/shard_map/project/pallas_call | solution.py:192
  29.8 0.0 copy-start.16
  29.8 0.0 copy-start.17
  29.8 0.0 copy-start.18
  29.8 0.0 copy-start.12
  29.9 0.0 copy-done.10
  29.9 0.0 copy-done.9
  29.9 0.1 multiply_reduce_fusion
  30.0 0.0 copy-done.11
  30.0 0.1 divide_multiply_fusion
  30.1 0.1 reshape.57
  30.2 0.1 copy.45
  30.3 0.1 reshape.58
  30.4 0.2 pad_maximum_fusion.heads_ref
  30.7 0.0 copy-done.16
  30.7 0.0 copy-done.17
  30.7 0.0 copy-done.18
  30.7 0.1 copy.46.par_ref
  30.8 0.0 copy-done.12
  30.8 0.1 reshape.63.gain_ref
  30.9 3.1 %copy-done = f32[7,64,4096]{2,1,0:T(8,128)S(1)} copy-done((f32[7,64,4096]{2,1,0:T(8,128)S(1)}, f32[7,64,4096]{2,1,0:T(8,128)}, u32[]{:S(2)}) %copy-start) | copy-done | bytes 7340056
  34.0 0.0 copy-start.1
  34.0 0.0 copy-start.8
  34.0 8.1 %state.1 = (f32[7,64,4096]{2,1,0:T(8,128)}, f32[7,64,64]{2,1,0:T(8,128)S(1)}) custom-call(f32[7,64,129]{2,1,0:T(8,128)S(1)} %pad_maximum_fusion.heads_ref, f32[7,512]{1,0:T(8,128)S(1)} %slice.33.bc_ref, f32[64,3]{1,0:T(8,128)S(1)} %copy.46.par_ref, f32[64,64]{1,0:T(8,128)S(1)} %reshape.63.gain_ref, f32[7,64,4096]{2,1,0:T(8,128)S(1)} %copy-done), custom_call_target="tpu_custom_call" | custom-call | tf_op jit(solution)/shard_map/state/pallas_call | solution.py:276
  42.1 0.1 reshape.61
  42.2 0.0 copy-done.14
  42.3 0.0 copy-done.13
  42.3 0.1 copy.47.ids_ref
  42.4 0.0 copy-done.19
  42.4 0.1 copy.48.prob_ref
  42.5 0.1 copy.49.score_ref
  42.6 0.0 copy-done.1
  42.6 1.6 %copy-done.2 = bf16[1,2048,512]{2,1,0:T(8,128)(2,1)S(1)} copy-done((bf16[1,2048,512]{2,1,0:T(8,128)(2,1)S(1)}, bf16[1,2048,512]{2,1,0:T(8,128)(2,1)}, u32[]{:S(2)}) %copy-start.2) | copy-done | bytes 2097176
  44.2 1.2 %copy-done.3 = bf16[4096,128]{1,0:T(8,128)(2,1)S(1)} copy-done((bf16[4096,128]{1,0:T(8,128)(2,1)S(1)}, bf16[4096,128]{1,0:T(8,128)(2,1)}, u32[]{:S(2)}) %copy-start.3) | copy-done | bytes 1048600
  45.4 36.4 %experts.1 = bf16[7,2048]{1,0:T(8,128)(2,1)S(1)} custom-call(bf16[8,4096]{1,0:T(8,128)(2,1)S(1)} %pad.9.y_ref, bf16[128,2048]{1,0:T(8,128)(2,1)S(1)} %get-tuple-element.15.hid_ref, bf16[7,2048]{1,0:T(8,128)(2,1)S(1)} %copy-done.8, s32[7,4]{1,0:T(8,128)S(1)} %copy.47.ids_ref, f32[7,1]{1,0:T(8,128)S(1)} %copy.48.prob_ref, f32[7,4]{1,0:T(8,128)S(1)} %copy.49.score_ref, ...), custom_call_target="tpu_custom_call" | custom-call | tf_op jit(solution)/shard_map/experts/pallas_call | solution.py:436
  81.8 0.1 maximum_maximum_fusion
  81.9 0.7 slice.34
  82.6 0.6 copy.51
  (27 shorter events, 0.1 us)
Async XLA Ops:
  4.2 1.2 %copy-start.4 = (bf16[2048,256]{1,0:T(8,128)(2,1)S(1)}, bf16[2048,256]{1,0:T(8,128)(2,1)}, u32[]{:S(2)}) copy-start(bf16[2048,256]{1,0:T(8,128)(2,1)} %z_any.1) | copy-start | bytes 3145732
  5.4 1.2 %copy-start.5 = (bf16[2048,256]{1,0:T(8,128)(2,1)S(1)}, bf16[2048,256]{1,0:T(8,128)(2,1)}, u32[]{:S(2)}) copy-start(bf16[2048,256]{1,0:T(8,128)(2,1)} %x_any.1) | copy-start | bytes 3145732
  6.7 1.2 %copy-start.6 = (bf16[2048,256]{1,0:T(8,128)(2,1)S(1)}, bf16[2048,256]{1,0:T(8,128)(2,1)}, u32[]{:S(2)}) copy-start(bf16[2048,256]{1,0:T(8,128)(2,1)} %b_any.1) | copy-start | bytes 3145732
  7.9 1.2 %copy-start.7 = (bf16[2048,256]{1,0:T(8,128)(2,1)S(1)}, bf16[2048,256]{1,0:T(8,128)(2,1)}, u32[]{:S(2)}) copy-start(bf16[2048,256]{1,0:T(8,128)(2,1)} %c_any.1) | copy-start | bytes 3145732
  9.1 20.7 %copy-start.10 = (bf16[4,4608]{1,0:T(4,128)(2,1)S(1)}, bf16[4,4608]{1,0:T(4,128)(2,1)}, u32[]{:S(2)}) copy-start(bf16[4,4608]{1,0:T(4,128)(2,1)} %param.35) | copy-start | bytes 110596
  9.1 20.8 %copy-start.9 = (bf16[7,3,4608]{2,0,1:T(8,128)(2,1)S(1)}, bf16[7,3,4608]{2,0,1:T(8,128)(2,1)}, u32[]{:S(2)}) copy-start(bf16[7,3,4608]{2,0,1:T(8,128)(2,1)} %param.25) | copy-start | bytes 580612
  9.1 20.9 %copy-start.11 = (bf16[4608]{0:T(1024)(128)(2,1)S(1)}, bf16[4608]{0:T(1024)(128)(2,1)}, u32[]{:S(2)}) copy-start(bf16[4608]{0:T(1024)(128)(2,1)} %param.36) | copy-start | bytes 27652
  29.8 0.9 %copy-start.16 = (f32[64]{0:T(128)S(1)}, f32[64]{0:T(128)}, u32[]{:S(2)}) copy-start(f32[64]{0:T(128)} %param.39) | copy-start | bytes 772
  29.8 0.9 %copy-start.17 = (f32[64]{0:T(128)S(1)}, f32[64]{0:T(128)}, u32[]{:S(2)}) copy-start(f32[64]{0:T(128)} %param.38) | copy-start | bytes 772
  29.8 0.9 %copy-start.18 = (f32[64]{0:T(128)S(1)}, f32[64]{0:T(128)}, u32[]{:S(2)}) copy-start(f32[64]{0:T(128)} %param.37) | copy-start | bytes 772
  29.8 1.0 %copy-start.12 = (bf16[4096]{0:T(1024)(128)(2,1)S(1)}, bf16[4096]{0:T(1024)(128)(2,1)}, u32[]{:S(2)}) copy-start(bf16[4096]{0:T(1024)(128)(2,1)} %param.40) | copy-start | bytes 24580
  30.9 3.1 %copy-start = (f32[7,64,4096]{2,1,0:T(8,128)S(1)}, f32[7,64,4096]{2,1,0:T(8,128)}, u32[]{:S(2)}) copy-start(f32[7,64,4096]{2,1,0:T(8,128)} %st_ref.1) | copy-start | bytes 22020100
  34.0 8.3 %copy-start.14 = (bf16[2048]{0:T(1024)(128)(2,1)S(1)}, bf16[2048]{0:T(1024)(128)(2,1)}, u32[]{:S(2)}) copy-start(bf16[2048]{0:T(1024)(128)(2,1)} %param.42) | copy-start | bytes 12292
  34.0 8.3 %copy-start.13 = (s32[7,4]{0,1:T(4,128)S(1)}, s32[7,4]{0,1:T(4,128)}, u32[]{:S(2)}) copy-start(s32[7,4]{0,1:T(4,128)} %param.26) | copy-start | bytes 340
  34.0 8.4 %copy-start.19 = (f32[7]{0:T(128)S(1)}, f32[7]{0:T(128)}, u32[]{:S(2)}) copy-start(f32[7]{0:T(128)} %param.27) | copy-start | bytes 88
  34.0 8.5 %copy-start.15 = (f32[7,4]{0,1:T(4,128)S(1)}, f32[7,4]{0,1:T(4,128)}, u32[]{:S(2)}) copy-start(f32[7,4]{0,1:T(4,128)} %param.28) | copy-start | bytes 340
  34.0 8.6 %copy-start.1 = (bf16[1,2048,512]{2,1,0:T(8,128)(2,1)S(1)}, bf16[1,2048,512]{2,1,0:T(8,128)(2,1)}, u32[]{:S(2)}) copy-start(bf16[1,2048,512]{2,1,0:T(8,128)(2,1)} %eg_any.1) | copy-start | bytes 6291460
  34.0 8.6 %copy-start.8 = (bf16[7,2048]{1,0:T(8,128)(2,1)S(1)}, bf16[7,2048]{1,0:T(8,128)(2,1)}, u32[]{:S(2)}) copy-start(bf16[7,2048]{1,0:T(8,128)(2,1)} %own_ref.1) | copy-start | bytes 86020
  42.6 1.6 %copy-start.2 = (bf16[1,2048,512]{2,1,0:T(8,128)(2,1)S(1)}, bf16[1,2048,512]{2,1,0:T(8,128)(2,1)}, u32[]{:S(2)}) copy-start(bf16[1,2048,512]{2,1,0:T(8,128)(2,1)} %eu_any.1) | copy-start | bytes 6291460
  44.2 1.2 %copy-start.3 = (bf16[4096,128]{1,0:T(8,128)(2,1)S(1)}, bf16[4096,128]{1,0:T(8,128)(2,1)}, u32[]{:S(2)}) copy-start(bf16[4096,128]{1,0:T(8,128)(2,1)} %ow_any.1) | copy-start | bytes 3145732

commit v2 on v1

--- a/solution.py
+++ b/solution.py
@@ -98,7 +98,7 @@
         copy.wait_send()
 
 
-def exchange(n, out_buf, in_buf, send, recv):
+def exchange_start(n, out_buf, in_buf, send, recv):
     me = lax.axis_index("ep")
     copies = []
     for d in range(1, n):
@@ -107,15 +107,25 @@
         copy.start()
         copies.append(copy)
     in_buf[me] = out_buf[me]
-    for copy in copies:
-        copy.wait_recv()
-    for copy in copies:
-        copy.wait_send()
+    return copies
+
+
+def spread(ref):
+    value = ref[...].astype(F32)
+    return jnp.concatenate([value[i : i + 1] for i in range(value.shape[0])], axis=1)
+
+
+def column(row):
+    size = row.shape[1]
+    at = lax.broadcasted_iota(jnp.int32, (size, size), 0)
+    to = lax.broadcasted_iota(jnp.int32, (size, size), 1)
+    return jnp.sum(jnp.where(at == to, row, jnp.zeros_like(row)), axis=1, keepdims=True)
 
 
 def project_kernel(
     n,
-    hid_ref,
+    own_ref,
+    ids_ref,
     gain_ref,
     z_any,
     x_any,
@@ -127,6 +137,7 @@
     x_ref,
     bc_ref,
     dt_ref,
+    hid_ref,
     hbuf,
     normed,
     zw,
@@ -139,8 +150,10 @@
     wsem,
     gs,
     gr,
-    es,
-    er,
+    xs,
+    xr,
+    zs,
+    zr,
 ):
     loads = [
         pltpu.make_async_copy(src, dst, wsem.at[i])
@@ -150,18 +163,29 @@
     ]
     for load in loads:
         load.start()
+    rows, width = own_ref.shape
+    ids = ids_ref[...].astype(F32)
+    pick = lax.broadcasted_iota(jnp.int32, (TOP, 128), 0)
+    lane = lax.broadcasted_iota(jnp.int32, (TOP, 128), 1)
+    spot = jnp.zeros((TOP, 128), F32)
+    for r in range(rows):
+        spot = spot + jnp.where(lane == TOP * r + pick, ids[:, r : r + 1] + 1.0, 0.0)
+    id_row = jnp.sum(spot, axis=0, keepdims=True) - 1.0
+    id_row = jnp.concatenate([id_row, jnp.full((1, width - 128), -1.0, F32)], axis=1)
+    hid_ref[...] = jnp.concatenate([own_ref[...].astype(F32), id_row], axis=0).astype(BF16)
     enter(n)
     me = lax.axis_index("ep")
     copies = gather_start(n, hid_ref, hbuf, gs, gr)
     hbuf[me] = hid_ref[...]
-    gain = gain_ref[...]
+    gain = spread(gain_ref)
     mine = rms_scale(hid_ref[...].astype(F32), gain).astype(BF16)
     for load in loads[:3]:
         load.wait()
     span = bw.shape[1]
     bc_ref[:, :span] = jnp.dot(mine, bw[...], preferred_element_type=F32).astype(BF16).astype(F32)
     bc_ref[:, span:] = jnp.dot(mine, cw[...], preferred_element_type=F32).astype(BF16).astype(F32)
-    dt_ref[...] = jnp.dot(mine, dw[...], preferred_element_type=F32).astype(BF16).astype(F32)
+    dt = lax.dot_general(mine, dw[...], (((1,), (1,)), ((), ())), preferred_element_type=F32)
+    dt_ref[...] = dt.astype(BF16).astype(F32)
     gather_finish(n, hid_ref, hbuf, gs, gr, copies)
     for j in range(0, n, 2):
         pair = jnp.concatenate([hbuf[j].astype(F32), hbuf[j + 1].astype(F32)], axis=0)
@@ -170,19 +194,23 @@
     for load in loads[3:]:
         load.wait()
     cols = zw.shape[1]
-    z_part = jnp.dot(normed[...], zw[...], preferred_element_type=F32)
-    x_part = jnp.dot(normed[...], xw[...], preferred_element_type=F32)
-    for j in range(n):
-        out_buf[j, :, :cols] = z_part[j * ROWS : (j + 1) * ROWS].astype(BF16)
-        out_buf[j, :, cols:] = x_part[j * ROWS : (j + 1) * ROWS].astype(BF16)
-    exchange(n, out_buf, in_buf, es, er)
-    for j in range(n):
-        z_ref[:, j * cols : (j + 1) * cols] = in_buf[j, :, :cols].astype(F32)
-        x_ref[:, j * cols : (j + 1) * cols] = in_buf[j, :, cols:].astype(F32)
-
-
-def project(n, hid8, first_gain, z_weight, x_weight, b_weight, c_weight, dt_weight):
-    width = hid8.shape[1]
+    flights = []
+    for h, (weight, send, recv) in enumerate([(xw, xs, xr), (zw, zs, zr)]):
+        part = jnp.dot(normed[...], weight[...], preferred_element_type=F32)
+        for j in range(n):
+            out_buf[h, j] = part[j * ROWS : (j + 1) * ROWS].astype(BF16)
+        flights.append(exchange_start(n, out_buf.at[h], in_buf.at[h], send, recv))
+    for h, ref in enumerate([x_ref, z_ref]):
+        for copy in flights[h]:
+            copy.wait_recv()
+        for j in range(n):
+            ref[:, j * cols : (j + 1) * cols] = in_buf[h, j].astype(F32)
+    for copy in flights[0] + flights[1]:
+        copy.wait_send()
+
+
+def project(n, hidden, ids, first_gain, z_weight, x_weight, b_weight, c_weight, dt_weight):
+    width = hidden.shape[1]
     cols = z_weight.shape[1]
     inner = n * cols
     span = b_weight.shape[1]
@@ -196,11 +224,12 @@
             jax.ShapeDtypeStruct((ROWS, inner), F32),
             jax.ShapeDtypeStruct((ROWS, inner), F32),
             jax.ShapeDtypeStruct((ROWS, 2 * span), F32),
-            jax.ShapeDtypeStruct((ROWS, dt_weight.shape[1]), F32),
+            jax.ShapeDtypeStruct((ROWS, dt_weight.shape[0]), F32),
         ),
-        in_specs=[vm, vm] + [hbm] * 5,
+        in_specs=[vm] * 3 + [hbm] * 5,
         out_specs=(vm,) * 5,
         scratch_shapes=[
+            pltpu.VMEM((ROWS, width), BF16),
             pltpu.VMEM((n, ROWS, width), BF16),
             pltpu.VMEM((n * ROWS, width), BF16),
             pltpu.VMEM(z_weight.shape, BF16),
@@ -208,19 +237,16 @@
             pltpu.VMEM(b_weight.shape, BF16),
             pltpu.VMEM(c_weight.shape, BF16),
             pltpu.VMEM(dt_weight.shape, BF16),
-            pltpu.VMEM((n, ROWS, 2 * cols), BF16),
-            pltpu.VMEM((n, ROWS, 2 * cols), BF16),
+            pltpu.VMEM((2, n, ROWS, cols), BF16),
+            pltpu.VMEM((2, n, ROWS, cols), BF16),
             dma((5,)),
-            dma((n - 1,)),
-            dma((n - 1,)),
-            dma((n - 1,)),
-            dma((n - 1,)),
-        ],
+        ]
+        + [dma((n - 1,))] * 6,
         compiler_params=pltpu.CompilerParams(
-            collective_id=0, has_side_effects=True, vmem_limit_bytes=40 << 20
+            collective_id=0, has_side_effects=True, vmem_limit_bytes=60 << 20
         ),
         name="project",
-    )(hid8, first_gain[None, :], z_weight, x_weight, b_weight, c_weight, dt_weight)
+    )(hidden, ids.T, first_gain.reshape(-1, 128), z_weight, x_weight, b_weight, c_weight, dt_weight)
 
 
 def state_kernel(heads_ref, bc_ref, par_ref, gain_ref, st_ref, out_ref, y_ref):
@@ -291,7 +317,7 @@
             pl.BlockSpec((1, HEADS, flat), lambda s: (s, 0, 0)),
             pl.BlockSpec((1, HEADS, HEAD_DIM), lambda s: (s, 0, 0)),
         ),
-        compiler_params=pltpu.CompilerParams(vmem_limit_bytes=40 << 20),
+        compiler_params=pltpu.CompilerParams(vmem_limit_bytes=60 << 20),
         name="state",
     )(heads, bc, par, gain, state_in)
 
@@ -331,6 +357,8 @@
     pr,
     es,
     er,
+    fs,
+    fr,
 ):
     loads = [
         pltpu.make_async_copy(src, dst, wsem.at[i])
@@ -360,13 +388,14 @@
     rows = out_ref.shape[0]
     col = lax.broadcasted_iota(jnp.int32, (rows, n * cap), 1)
     score = score_ref[...]
-    share = prob_ref[...] * score / jnp.sum(score, axis=1, keepdims=True)
+    share = prob_ref[...] * score / jnp.sum(score, axis=0, keepdims=True)
+    ids = ids_ref[...].astype(F32)
     weight = jnp.zeros((rows, n * cap), F32)
     used = jnp.zeros((rows, n * cap), F32)
     for pick in range(TOP):
-        hit = (ids_ref[:, pick : pick + 1] == col // cap).astype(F32)
+        hit = (column(ids[pick : pick + 1]) == (col // cap).astype(F32)).astype(F32)
         used = used + hit
-        weight = weight + hit * share[:, pick : pick + 1]
+        weight = weight + hit * column(share[pick : pick + 1])
     row_id = lax.broadcasted_iota(jnp.int32, (rows, n * cap), 0)
     rank = jnp.zeros((rows, n * cap), F32)
     for r in range(rows - 1):
@@ -386,10 +415,9 @@
     for j in range(n):
         at = slice(j * cols, (j + 1) * cols)
         mixed[:, at] = (hid_ref[:, at].astype(F32) + pbuf[j].astype(F32)).astype(BF16)
+    gain = spread(gain_ref)
     for j in range(0, total, 16):
-        normed[j : j + 16, :] = rms_scale(mixed[j : j + 16, :].astype(F32), gain_ref[...]).astype(
-            BF16
-        )
+        normed[j : j + 16, :] = rms_scale(mixed[j : j + 16, :].astype(F32), gain).astype(BF16)
     for load in loads[1:]:
         load.wait()
     for j in range(0, eg.shape[1], 256):
@@ -398,29 +426,40 @@
         up = jnp.dot(normed[...], eu[:, at], preferred_element_type=F32)
         act[:, at] = (jax.nn.silu(gate) * up).astype(BF16)
     width = eo.shape[1]
+    wide = width // 2
+    tile = 256
 
     def down(i, carry):
-        at = pl.ds(pl.multiple_of(i * 256, 256), 256)
+        at = pl.ds(pl.multiple_of(i * tile, tile), tile)
         part = jnp.dot(act[...], ed[:, at], preferred_element_type=F32).astype(BF16)
         eo[:, at] = jnp.dot(select, part, preferred_element_type=F32)
         return carry
 
-    lax.fori_loop(0, width // 256, down, 0)
-    for j in range(n):
-        out_buf[j] = eo[j * ROWS : j * ROWS + cap, :].astype(BF16)
-    exchange(n, out_buf, in_buf, es, er)
-    per = ROWS // cap
-    for j in range(0, n, per):
-        eo[j * cap : (j + per) * cap, :] = jnp.concatenate(
-            [in_buf[j + i].astype(F32) for i in range(per)], axis=0
-        )
-    back = eo[: n * cap, :].astype(BF16)
-    moe = jnp.dot(high, back, preferred_element_type=F32) + jnp.dot(
-        low, back, preferred_element_type=F32
-    )
+    flights = []
+    for h, (send, recv) in enumerate([(es, er), (fs, fr)]):
+        lax.fori_loop(h * wide // tile, (h + 1) * wide // tile, down, 0)
+        for j in range(n):
+            out_buf[h, j] = eo[j * ROWS : j * ROWS + cap, h * wide : (h + 1) * wide].astype(BF16)
+        flights.append(exchange_start(n, out_buf.at[h], in_buf.at[h], send, recv))
     start = pl.multiple_of(me * ROWS, ROWS)
     eo[...] = mixed[...].astype(F32)
-    out_ref[...] = (eo[pl.ds(start, ROWS), :][:rows] + moe).astype(BF16)
+    base = eo[pl.ds(start, ROWS), :][:rows]
+    per = ROWS // cap
+    for h in range(2):
+        for copy in flights[h]:
+            copy.wait_recv()
+        for j in range(0, n, per):
+            eo[j * cap : (j + per) * cap, :wide] = jnp.concatenate(
+                [in_buf[h, j + i].astype(F32) for i in range(per)], axis=0
+            )
+        back = eo[: n * cap, :wide].astype(BF16)
+        moe = jnp.dot(high, back, preferred_element_type=F32) + jnp.dot(
+            low, back, preferred_element_type=F32
+        )
+        at = slice(h * wide, (h + 1) * wide)
+        out_ref[:, at] = (base[:, at] + moe).astype(BF16)
+    for copy in flights[0] + flights[1]:
+        copy.wait_send()
 
 
 def experts(
@@ -450,23 +489,23 @@
             pltpu.VMEM(gate_w.shape[1:], BF16),
             pltpu.VMEM(up_w.shape[1:], BF16),
             pltpu.VMEM(down_w.shape[1:], BF16),
-            pltpu.VMEM((n, cap, width), BF16),
-            pltpu.VMEM((n, cap, width), BF16),
+            pltpu.VMEM((2, n, cap, width // 2), BF16),
+            pltpu.VMEM((2, n, cap, width // 2), BF16),
             dma((4,)),
         ]
-        + [dma((n - 1,))] * 6,
+        + [dma((n - 1,))] * 8,
         compiler_params=pltpu.CompilerParams(
-            collective_id=1, has_side_effects=True, vmem_limit_bytes=48 << 20
+            collective_id=1, has_side_effects=True, vmem_limit_bytes=60 << 20
         ),
         name="experts",
     )(
         y8,
         hid_all,
         hidden,
-        ids,
-        prob[:, None],
-        score,
-        second_gain[None, :],
+        ids.T,
+        prob[None, :],
+        score.T,
+        second_gain.reshape(-1, 128),
         out_weight,
         gate_w,
         up_w,
@@ -502,18 +541,15 @@
     n = lax.axis_size("ep")
     rows, width = hidden.shape
     inner = HEADS * HEAD_DIM
-    id_row = jnp.pad(
-        expert_ids.astype(BF16).reshape(1, -1),
-        ((0, 0), (0, width - rows * TOP)),
-        constant_values=-1,
-    )
-    hid8 = jnp.concatenate([hidden, id_row], axis=0)
     hid_all, z8, x8, bc8, dt8 = project(
-        n, hid8, first_gain, z_weight, x_weight, b_weight, c_weight, dt_weight
+        n, hidden, expert_ids, first_gain, z_weight, x_weight, b_weight, c_weight, dt_weight.T
     )
     fresh = jnp.concatenate([x8[:rows], bc8[:rows]], axis=1).astype(BF16)
-    window = jnp.concatenate([conv_state, fresh[:, None, :]], axis=1)
-    summed = jnp.sum(window.astype(F32) * conv_weight.astype(F32)[None], axis=1)
+    taps = conv_weight.astype(F32)
+    held = conv_state.shape[1]
+    summed = jnp.sum(conv_state.astype(F32) * taps[None, :held], axis=1)
+    summed = summed + fresh.astype(F32) * taps[held][None]
+    conv_out = jnp.concatenate([conv_state[:, 1:], fresh[:, None, :]], axis=1)
     active = jax.nn.silu(summed + conv_bias.astype(F32)[None, :])
     heads = jnp.concatenate(
         [
@@ -549,7 +585,7 @@
         expert_up,
         expert_down,
     )
-    return (layer_out, state_out, window[:, 1:, :])
+    return (layer_out, state_out, conv_out)
 
 
 def solution(mesh):

time: 83.8 us -> 82.1 us (0.980)
  local copies, waits for them, and re-layouts: 15.3 us -> 7.02 us
  Pallas kernels: 65.1 us -> 70.9 us
  other arithmetic: 1.9 us -> 2.81 us
    unnamed x44 -> x21, local copies, waits for them, and re-layouts: 12.9 us -> 1.43 us
    pallas_call x1, Pallas kernels: 20.6 us -> 23.3 us  [project(): pl.pallas_call(functools.partial(project_kernel, n), out_shape=(jax.Shape...]
    pallas_call x1, Pallas kernels: 8.06 us -> 10.5 us  [state_update(): pl.pallas_call(state_kernel, grid=(rows,), out_shape=(jax.ShapeDtypeStruc...]
    slice x1 -> x6, local copies, waits for them, and re-layouts: 0.7 us -> 1.77 us  [the longest x2 1.7 us: body(): fresh = jnp.concatenate([x8[:rows], bc8[:rows]], axis=1).astype(BF16)]
    convert_element_type x1, other arithmetic: 0.02 us -> 0.96 us  [body(): y_heads.astype(BF16).reshape(rows, inner)]
where the time goes in v2:
time: 82.1 us; the launch traced here: 81.6 us
  Pallas kernels  70.9 us (86%)
  local copies, waits for them, and re-layouts  7.02 us (9%)
  other arithmetic  2.81 us (3%)
  between operations  0.85 us (1%)
    pallas_call x1, Pallas kernels, experts(): pl.pallas_call(functools.partial(expert_kernel, n, cap), out_shape=jax.Sh...  37.1 us
    pallas_call x1, Pallas kernels, project(): pl.pallas_call(functools.partial(project_kernel, n), out_shape=(jax.Shape...  23.3 us
    pallas_call x1, Pallas kernels, state_update(): pl.pallas_call(state_kernel, grid=(rows,), out_shape=(jax.ShapeDtypeStruc...  10.5 us
    slice x2, local copies, waits for them, and re-layouts, body(): fresh = jnp.concatenate([x8[:rows], bc8[:rows]], axis=1).astype(BF16)  1.7 us

profile of v2, /device:TPU:0, one launch (start us, length us, event | category | flops | bytes accessed | tf_op | source)
XLA Modules:
  0.0 81.6 jit_solution(12540154369279419411)
XLA Ops:
  0.6 0.0 copy-start.1
  0.6 0.0 copy-start
  0.7 0.0 copy-start.5
  0.7 23.3 %project.1 = (bf16[128,2048]{1,0:T(8,128)(2,1)}, f32[8,4096]{1,0:T(8,128)}, f32[8,4096]{1,0:T(8,128)}, f32[8,512]{1,0:T(8,128)}, f32[8,64]{1,0:T(8,128)}) custom-call(bf16[7,2048]{1,0:T(8,128)(2,1)} %own_ref.3, s32[4,7]{1,0:T(4,128)} %bitcast.18, bf16[16,128]{1,0:T(8,128)(2,1)} %bitcast.20, bf16[2048,256]{1,0:T(8,128)(2,1)} %z_any.1, ...), custom_call_target="tpu_custom_call" | custom-call | tf_op jit(solution)/shard_map/project/pallas_call | solution.py:220
  24.0 0.0 copy-start.3
  24.0 0.0 copy-start.7
  24.0 0.0 copy-start.8
  24.0 0.0 copy-start.9
  24.0 0.0 copy-start.6
  24.0 1.0 %slice.44 = bf16[7,4096]{1,0:T(8,128)(2,1)S(1)} slice(f32[8,4096]{1,0:T(8,128)} %get-tuple-element.10), slice={[0:7], [0:4096]} | slice | bytes 114688 | tf_op jit(solution)/shard_map/slice | solution.py:547
  25.0 0.7 slice.45
  25.7 0.0 copy-done.1
  25.7 0.0 copy-done
  25.8 0.1 multiply_reduce_fusion
  25.8 0.1 slice_reduce_fusion
  25.9 0.0 copy-done.5
  25.9 0.1 divide_multiply_fusion
  26.0 0.1 reshape.60
  26.1 0.7 slice_bitcast_fusion
  26.8 0.1 copy.33
  26.9 0.0 copy-done.3
  26.9 0.1 reshape.61
  27.0 1.0 %pad_maximum_fusion.heads_ref = f32[7,64,129]{2,1,0:T(8,128)} fusion(f32[7,64,1]{2,1,0:T(8,128)S(1)} %copy.33, f32[7,64,64]{2,1,0:T(8,128)S(1)} %reshape.61, f32[7,64,64]{2,1,0:T(8,128)S(1)} %reshape.60), kind=kLoop, calls=%fused_computation | loop fusion | flops 115584 | bytes 462336 | tf_op jit(solution)/shard_map/concatenate | solution.py:554
  28.0 0.6 slice.39.bc_ref
  28.6 0.0 copy-done.7
  28.6 0.0 copy-done.8
  28.6 0.0 copy-done.9
  28.6 0.7 copy.34.par_ref
  29.3 0.0 copy-done.6
  29.4 0.7 reshape.67.gain_ref
  30.0 10.5 %state.1 = (f32[7,64,4096]{2,1,0:T(8,128)}, f32[7,64,64]{2,1,0:T(8,128)}) custom-call(f32[7,64,129]{2,1,0:T(8,128)} %pad_maximum_fusion.heads_ref, f32[7,512]{1,0:T(8,128)} %slice.39.bc_ref, f32[64,3]{1,0:T(8,128)} %copy.34.par_ref, f32[64,64]{1,0:T(8,128)} %reshape.67.gain_ref, f32[7,64,4096]{2,1,0:T(8,128)} %st_ref.1), custom_call_target="tpu_custom_call" | custom-call | tf_op jit(solution)/shard_map/state/pallas_call | solution.py:302
  40.6 1.0 %convert_element_type.30 = bf16[7,64,64]{2,1,0:T(8,128)(2,1)S(1)} convert(f32[7,64,64]{2,1,0:T(8,128)} %get-tuple-element.14) | non-fusion elementwise | flops 28672 | bytes 172032 | tf_op jit(solution)/shard_map/convert_element_type | solution.py:570
  41.5 0.1 reshape.64
  41.7 0.6 pad.4.y_ref
  42.3 0.0 copy-start.2
  42.3 0.0 copy-start.4
  42.3 0.0 slice-start
  42.3 37.1 %experts.1 = bf16[7,2048]{1,0:T(8,128)(2,1)} custom-call(bf16[8,4096]{1,0:T(8,128)(2,1)} %pad.4.y_ref, bf16[128,2048]{1,0:T(8,128)(2,1)} %get-tuple-element.15.hid_ref, bf16[7,2048]{1,0:T(8,128)(2,1)} %own_ref.3, s32[4,7]{1,0:T(4,128)} %bitcast.19, f32[1,7]{1,0:T(1,128)} %bitcast.23, f32[4,7]{1,0:T(4,128)} %bitcast.22, bf16[16,128]{1,0:T(8,128)(2,1)} %bitcast.21, ...), custom_call_target="tpu_custom_call" | custom-call | tf_op jit(solution)/shard_map/experts/pallas_call | solution.py:475
  79.4 0.0 copy-done.2
  79.4 0.0 copy-done.4
  79.4 0.0 slice-done
  79.5 0.7 maximum_maximum_fusion
  80.2 1.4 %copy.36 = bf16[7,2048]{1,0:T(8,128)(2,1)} copy(bf16[7,2048]{1,0:T(8,128)(2,1)} %experts.1) | data formatting | bytes 57344
  (7 shorter events, 0.1 us)
Async XLA Ops:
  0.6 25.1 %copy-start.1 = (bf16[4,4608]{1,0:T(4,128)(2,1)S(1)}, bf16[4,4608]{1,0:T(4,128)(2,1)}, u32[]{:S(2)}) copy-start(bf16[4,4608]{1,0:T(4,128)(2,1)} %param.35) | copy-start | bytes 110596
  0.6 25.1 %copy-start = (bf16[7,3,4608]{2,0,1:T(8,128)(2,1)S(1)}, bf16[7,3,4608]{2,0,1:T(8,128)(2,1)}, u32[]{:S(2)}) copy-start(bf16[7,3,4608]{2,0,1:T(8,128)(2,1)} %param.25) | copy-start | bytes 580612
  0.7 25.2 %copy-start.5 = (bf16[4608]{0:T(1024)(128)(2,1)S(1)}, bf16[4608]{0:T(1024)(128)(2,1)}, u32[]{:S(2)}) copy-start(bf16[4608]{0:T(1024)(128)(2,1)} %param.36) | copy-start | bytes 27652
  24.0 3.0 %copy-start.3 = (f32[8,4096]{1,0:T(8,128)S(1)}, f32[8,4096]{1,0:T(8,128)}, u32[]{:S(2)}) copy-start(f32[8,4096]{1,0:T(8,128)} %get-tuple-element.12) | copy-start | bytes 393220
  24.0 4.6 %copy-start.7 = (f32[64]{0:T(128)S(1)}, f32[64]{0:T(128)}, u32[]{:S(2)}) copy-start(f32[64]{0:T(128)} %param.39) | copy-start | bytes 772
  24.0 4.6 %copy-start.8 = (f32[64]{0:T(128)S(1)}, f32[64]{0:T(128)}, u32[]{:S(2)}) copy-start(f32[64]{0:T(128)} %param.38) | copy-start | bytes 772
  24.0 4.6 %copy-start.9 = (f32[64]{0:T(128)S(1)}, f32[64]{0:T(128)}, u32[]{:S(2)}) copy-start(f32[64]{0:T(128)} %param.37) | copy-start | bytes 772
  24.0 5.3 %copy-start.6 = (bf16[4096]{0:T(1024)(128)(2,1)S(1)}, bf16[4096]{0:T(1024)(128)(2,1)}, u32[]{:S(2)}) copy-start(bf16[4096]{0:T(1024)(128)(2,1)} %param.40) | copy-start | bytes 24580
  42.3 37.1 %copy-start.2 = (f32[8,4096]{1,0:T(8,128)S(1)}, f32[8,4096]{1,0:T(8,128)}, u32[]{:S(2)}) copy-start(f32[8,4096]{1,0:T(8,128)} %get-tuple-element.10) | copy-start | bytes 393220
  42.3 37.1 %copy-start.4 = (f32[8,512]{1,0:T(8,128)S(1)}, f32[8,512]{1,0:T(8,128)}, u32[]{:S(2)}) copy-start(f32[8,512]{1,0:T(8,128)} %get-tuple-element.11) | copy-start | bytes 49156
  42.3 37.1 %slice-start = ((bf16[7,3,4608]{2,0,1:T(8,128)(2,1)}), bf16[7,2,4608]{2,0,1:T(8,128)(2,1)S(1)}, s32[]{:S(2)}) async-start(bf16[7,3,4608]{2,0,1:T(8,128)(2,1)} %param.25), calls=%async_computation | async-start | bytes 294912 | tf_op jit(solution)/shard_map/slice | solution.py:552

commit v3 on v2

--- a/solution.py
+++ b/solution.py
@@ -317,7 +317,7 @@
             pl.BlockSpec((1, HEADS, flat), lambda s: (s, 0, 0)),
             pl.BlockSpec((1, HEADS, HEAD_DIM), lambda s: (s, 0, 0)),
         ),
-        compiler_params=pltpu.CompilerParams(vmem_limit_bytes=60 << 20),
+        compiler_params=pltpu.CompilerParams(vmem_limit_bytes=40 << 20),
         name="state",
     )(heads, bc, par, gain, state_in)
 

time: 82.1 us -> 78.9 us (0.961)
  Pallas kernels: 70.9 us -> 68.3 us
  other arithmetic: 2.81 us -> 1.09 us
  local copies, waits for them, and re-layouts: 7.02 us -> 8.27 us
    unnamed x21 -> x23, local copies, waits for them, and re-layouts: 1.43 us -> 4.51 us
    pallas_call x1, Pallas kernels: 10.5 us -> 8.03 us  [state_update(): pl.pallas_call(state_kernel, grid=(rows,), out_shape=(jax.ShapeDtypeStruc...]
    convert_element_type x1, other arithmetic: 0.96 us -> 0.02 us  [body(): y_heads.astype(BF16).reshape(rows, inner)]
where the time goes in v3:
time: 78.9 us; the launch traced here: 78.6 us
  Pallas kernels  68.3 us (87%)
  local copies, waits for them, and re-layouts  8.27 us (10%)
  other arithmetic  1.09 us (1%)
  between operations  0.88 us (1%)
    pallas_call x1, Pallas kernels, experts(): pl.pallas_call(functools.partial(expert_kernel, n, cap), out_shape=jax.Sh...  37 us
    pallas_call x1, Pallas kernels, project(): pl.pallas_call(functools.partial(project_kernel, n), out_shape=(jax.Shape...  23.3 us
    pallas_call x1, Pallas kernels, state_update(): pl.pallas_call(state_kernel, grid=(rows,), out_shape=(jax.ShapeDtypeStruc...  8.03 us
    unnamed x23, local copies, waits for them, and re-layouts  4.51 us
    slice x2, local copies, waits for them, and re-layouts, body(): fresh = jnp.concatenate([x8[:rows], bc8[:rows]], axis=1).astype(BF16)  1.7 us

profile of v3, /device:TPU:0, one launch (start us, length us, event | category | flops | bytes accessed | tf_op | source)
XLA Modules:
  0.0 78.6 jit_solution(9900848179019110526)
XLA Ops:
  0.6 0.0 copy-start.2
  0.6 0.0 copy-start.1
  0.7 0.0 copy-start.6
  0.7 23.3 %project.1 = (bf16[128,2048]{1,0:T(8,128)(2,1)}, f32[8,4096]{1,0:T(8,128)}, f32[8,4096]{1,0:T(8,128)}, f32[8,512]{1,0:T(8,128)}, f32[8,64]{1,0:T(8,128)}) custom-call(bf16[7,2048]{1,0:T(8,128)(2,1)} %own_ref.3, s32[4,7]{1,0:T(4,128)} %bitcast.18, bf16[16,128]{1,0:T(8,128)(2,1)} %bitcast.20, bf16[2048,256]{1,0:T(8,128)(2,1)} %z_any.1, ...), custom_call_target="tpu_custom_call" | custom-call | tf_op jit(solution)/shard_map/project/pallas_call | solution.py:220
  23.9 0.0 copy-start.4
  23.9 0.0 copy-start.8
  24.0 0.0 copy-start.9
  24.0 0.0 copy-start.10
  24.0 0.0 copy-start.7
  24.0 1.0 %slice.44 = bf16[7,4096]{1,0:T(8,128)(2,1)S(1)} slice(f32[8,4096]{1,0:T(8,128)} %get-tuple-element.10), slice={[0:7], [0:4096]} | slice | bytes 114688 | tf_op jit(solution)/shard_map/slice | solution.py:547
  25.0 0.7 slice.45
  25.7 0.0 copy-done.2
  25.7 0.0 copy-done.1
  25.7 0.1 multiply_reduce_fusion
  25.8 0.1 slice_reduce_fusion
  25.9 0.0 copy-done.6
  25.9 0.1 divide_multiply_fusion
  26.0 0.1 reshape.60
  26.1 0.7 slice_bitcast_fusion
  26.7 0.1 copy.33
  26.9 0.0 copy-done.4
  26.9 0.1 reshape.61
  27.0 0.2 pad_maximum_fusion.heads_ref
  27.2 0.0 copy-done.8
  27.2 0.0 copy-done.9
  27.2 0.0 copy-done.10
  27.3 0.1 copy.34.par_ref
  27.4 0.0 copy-done.7
  27.4 0.1 reshape.67.gain_ref
  27.4 0.0 copy-start
  27.4 3.1 %copy-done = f32[7,64,4096]{2,1,0:T(8,128)S(1)} copy-done((f32[7,64,4096]{2,1,0:T(8,128)S(1)}, f32[7,64,4096]{2,1,0:T(8,128)}, u32[]{:S(2)}) %copy-start) | copy-done | bytes 7340056
  30.5 8.0 %state.1 = (f32[7,64,4096]{2,1,0:T(8,128)}, f32[7,64,64]{2,1,0:T(8,128)S(1)}) custom-call(f32[7,64,129]{2,1,0:T(8,128)S(1)} %pad_maximum_fusion.heads_ref, f32[7,512]{1,0:T(8,128)S(1)} %slice.39.bc_ref, f32[64,3]{1,0:T(8,128)S(1)} %copy.34.par_ref, f32[64,64]{1,0:T(8,128)S(1)} %reshape.67.gain_ref, f32[7,64,4096]{2,1,0:T(8,128)S(1)} %copy-done), custom_call_target="tpu_custom_call" | custom-call | tf_op jit(solution)/shard_map/state/pallas_call | solution.py:302
  38.6 0.1 reshape.64
  38.7 0.6 pad.4.y_ref
  39.4 0.0 copy-start.3
  39.4 0.0 copy-start.5
  39.4 0.0 slice-start
  39.4 37.0 %experts.1 = bf16[7,2048]{1,0:T(8,128)(2,1)} custom-call(bf16[8,4096]{1,0:T(8,128)(2,1)} %pad.4.y_ref, bf16[128,2048]{1,0:T(8,128)(2,1)} %get-tuple-element.15.hid_ref, bf16[7,2048]{1,0:T(8,128)(2,1)} %own_ref.3, s32[4,7]{1,0:T(4,128)} %bitcast.19, f32[1,7]{1,0:T(1,128)} %bitcast.23, f32[4,7]{1,0:T(4,128)} %bitcast.22, bf16[16,128]{1,0:T(8,128)(2,1)} %bitcast.21, ...), custom_call_target="tpu_custom_call" | custom-call | tf_op jit(solution)/shard_map/experts/pallas_call | solution.py:475
  76.4 0.0 copy-done.3
  76.5 0.0 copy-done.5
  76.5 0.0 slice-done
  76.5 0.7 maximum_maximum_fusion
  77.2 1.4 %copy.36 = bf16[7,2048]{1,0:T(8,128)(2,1)} copy(bf16[7,2048]{1,0:T(8,128)(2,1)} %experts.1) | data formatting | bytes 57344
  (9 shorter events, 0.1 us)
Async XLA Ops:
  0.6 25.1 %copy-start.2 = (bf16[4,4608]{1,0:T(4,128)(2,1)S(1)}, bf16[4,4608]{1,0:T(4,128)(2,1)}, u32[]{:S(2)}) copy-start(bf16[4,4608]{1,0:T(4,128)(2,1)} %param.35) | copy-start | bytes 110596
  0.6 25.1 %copy-start.1 = (bf16[7,3,4608]{2,0,1:T(8,128)(2,1)S(1)}, bf16[7,3,4608]{2,0,1:T(8,128)(2,1)}, u32[]{:S(2)}) copy-start(bf16[7,3,4608]{2,0,1:T(8,128)(2,1)} %param.25) | copy-start | bytes 580612
  0.7 25.2 %copy-start.6 = (bf16[4608]{0:T(1024)(128)(2,1)S(1)}, bf16[4608]{0:T(1024)(128)(2,1)}, u32[]{:S(2)}) copy-start(bf16[4608]{0:T(1024)(128)(2,1)} %param.36) | copy-start | bytes 27652
  23.9 3.0 %copy-start.4 = (f32[8,4096]{1,0:T(8,128)S(1)}, f32[8,4096]{1,0:T(8,128)}, u32[]{:S(2)}) copy-start(f32[8,4096]{1,0:T(8,128)} %get-tuple-element.12) | copy-start | bytes 393220
  23.9 3.3 %copy-start.8 = (f32[64]{0:T(128)S(1)}, f32[64]{0:T(128)}, u32[]{:S(2)}) copy-start(f32[64]{0:T(128)} %param.39) | copy-start | bytes 772
  24.0 3.3 %copy-start.9 = (f32[64]{0:T(128)S(1)}, f32[64]{0:T(128)}, u32[]{:S(2)}) copy-start(f32[64]{0:T(128)} %param.38) | copy-start | bytes 772
  24.0 3.3 %copy-start.10 = (f32[64]{0:T(128)S(1)}, f32[64]{0:T(128)}, u32[]{:S(2)}) copy-start(f32[64]{0:T(128)} %param.37) | copy-start | bytes 772
  24.0 3.4 %copy-start.7 = (bf16[4096]{0:T(1024)(128)(2,1)S(1)}, bf16[4096]{0:T(1024)(128)(2,1)}, u32[]{:S(2)}) copy-start(bf16[4096]{0:T(1024)(128)(2,1)} %param.40) | copy-start | bytes 24580
  27.4 3.1 %copy-start = (f32[7,64,4096]{2,1,0:T(8,128)S(1)}, f32[7,64,4096]{2,1,0:T(8,128)}, u32[]{:S(2)}) copy-start(f32[7,64,4096]{2,1,0:T(8,128)} %st_ref.1) | copy-start | bytes 22020100
  39.4 37.1 %copy-start.3 = (f32[8,4096]{1,0:T(8,128)S(1)}, f32[8,4096]{1,0:T(8,128)}, u32[]{:S(2)}) copy-start(f32[8,4096]{1,0:T(8,128)} %get-tuple-element.10) | copy-start | bytes 393220
  39.4 37.1 %copy-start.5 = (f32[8,512]{1,0:T(8,128)S(1)}, f32[8,512]{1,0:T(8,128)}, u32[]{:S(2)}) copy-start(f32[8,512]{1,0:T(8,128)} %get-tuple-element.11) | copy-start | bytes 49156
  39.4 37.1 %slice-start = ((bf16[7,3,4608]{2,0,1:T(8,128)(2,1)}), bf16[7,2,4608]{2,0,1:T(8,128)(2,1)S(1)}, s32[]{:S(2)}) async-start(bf16[7,3,4608]{2,0,1:T(8,128)(2,1)} %param.25), calls=%async_computation | async-start | bytes 294912 | tf_op jit(solution)/shard_map/slice | solution.py:552
